TPU v7x, 32 devices: a whole 2x2x4 slice. The times are simulated.
32 devices in a mesh: grp: 2 (over y), fs: 4 (over z), tp: 4 (over x, core).
Axes of the slice: x: 2, y: 2, z: 4, core: 2. Of those that a mesh axis runs over, the one named last changes fastest.
Arguments:
- layer_input: bfloat16 [3072, 2048], P(('grp', 'fs'), 'tp'), parts along dimension 0, may hold values from -6 to 6
- first_gain: bfloat16 [1, 2048], P(None, 'tp'), may hold values from 0.099609375 to 1.8984375
- ffn_gate_w: bfloat16 [2048, 6144], P('fs', 'tp'), may hold values from -0.125 to 0.125
- ffn_up_w: bfloat16 [2048, 6144], P('fs', 'tp'), may hold values from -0.125 to 0.125
- ffn_down_w: bfloat16 [6144, 2048], P('tp', 'fs'), may hold values from -0.078125 to 0.078125
- mixer_gain: bfloat16 [1, 2048], P(None, 'tp'), may hold values from 0.099609375 to 1.8984375
- pool_in_w: bfloat16 [2048, 1024], P('fs', 'tp'), may hold values from -0.125 to 0.125
- mixer_gate_w: bfloat16 [2048, 2048], P('fs', 'tp'), may hold values from -0.125 to 0.125
- group_mix_w: bfloat16 [8, 128, 128], P('tp'), may hold values from -0.5 to 0.5
- pool_scale: float32 [1, 1024], P(None, 'tp'), may hold values from 0.1 to 1.9
- mixer_out_w: bfloat16 [1024, 2048], P('tp', 'fs'), may hold values from -0.1875 to 0.1875
- second_gain: bfloat16 [1, 2048], P(None, 'tp'), may hold values from 0.099609375 to 1.8984375
Outputs:
- layer_output: bfloat16 [3072, 2048], P(('grp', 'fs'), 'tp'), parts along dimension 0
There are 2 independent parts, one for each index of `grp`. A program takes and returns all parts, laid end to end along the dimension named above; an argument that names none is the same for every part. Nothing has to cross between parts.
All inputs are finite; a program needn't handle non-finite values.
Results may differ from a plain program's by a relative error of at most 0.015.
Values may be sent and summed in bfloat16 or wider, within the bound.
No kernel may reach another device: no remote copies, remote signals or barrier semaphores. Data moves between devices by JAX's collectives and lax.ppermute only.
A program may use at most 64 MiB of HBM per device.

v0:
```python
import jax
import jax.numpy as jnp
from jax import lax
from jax.sharding import PartitionSpec as P


def shift(size, step):
    return [(i, (i + step) % size) for i in range(size)]


def swap(size):
    return [(i, i ^ 1) for i in range(size)]


def per_device(
    layer_input,
    first_gain,
    ffn_gate_w,
    ffn_up_w,
    ffn_down_w,
    mixer_gain,
    pool_in_w,
    mixer_gate_w,
    group_mix_w,
    pool_scale,
    mixer_out_w,
    second_gain,
):
    n_grp, n_fs, n_tp = (lax.axis_size(name) for name in ("grp", "fs", "tp"))
    n_chip = n_tp // 2
    y, z, t = (lax.axis_index(name) for name in ("grp", "fs", "tp"))
    chip, core = (t // 2, t % 2)
    rows, shard = layer_input.shape
    width = shard * n_tp
    block = width // n_fs

    def pieces_of(weight, axis):
        part = weight.shape[axis] // n_grp
        own = [
            lax.dynamic_slice_in_dim(weight, (y - k) % n_grp * part, part, axis)
            for k in range(n_grp)
        ]
        gathered, current = ([own], own[0])
        for _ in range(n_fs - 1):
            current = lax.ppermute(current, "fs", shift(n_fs, 1))
            gathered.append(
                [current] + [lax.ppermute(current, "grp", shift(n_grp, k)) for k in range(1, n_grp)]
            )
        return gathered

    def absolute(weight, axis, split):
        gathered = pieces_of(weight, split)
        shape = list(weight.shape)
        shape[axis] *= n_fs
        whole = jnp.zeros(shape, weight.dtype)
        for s, parts in enumerate(gathered):
            for k, part in enumerate(parts):
                start = [0, 0]
                start[axis] = (z - s) % n_fs * weight.shape[axis]
                start[split] = start[split] + (y - k) % n_grp * part.shape[split]
                whole = lax.dynamic_update_slice(whole, part, start)
        return whole

    def gather_tp(value):
        pieces = [(t, value), (t ^ 1, lax.ppermute(value, "tp", swap(n_tp)))]
        for k in range(1, n_chip):
            far = lax.ppermute(value, "tp", shift(n_tp, 2 * k))
            source = (t - 2 * k) % n_tp
            pieces.append((source, far))
            pieces.append((source ^ 1, lax.ppermute(far, "tp", swap(n_tp))))
        whole = jnp.zeros((value.shape[0], value.shape[1] * n_tp), value.dtype)
        for source, piece in pieces:
            whole = lax.dynamic_update_slice(whole, piece, (0, source * value.shape[1]))
        return whole

    def scatter_tp(partial):

        def at(index):
            return lax.dynamic_slice_in_dim(partial, index * shard, shard, 1)

        total = None
        for k in list(range(1, n_chip)) + [0]:
            there = (chip + k) % n_chip * 2
            other = lax.ppermute(at(there + (1 - core)), "tp", swap(n_tp))
            pair = at(there + core).astype(jnp.float32) + other.astype(jnp.float32)
            if k:
                pair = lax.ppermute(pair.astype(jnp.bfloat16), "tp", shift(n_tp, 2 * k)).astype(
                    jnp.float32
                )
            total = pair if total is None else total + pair
        return total

    def norm_rows(values, gain):
        whole = gather_tp(values)
        gain_whole = lax.all_gather(gain, "tp", axis=1, tiled=True)
        widened = whole.astype(jnp.float32)
        scaled = (widened * gain_whole.astype(jnp.float32)).astype(jnp.bfloat16)
        factor = lax.rsqrt(jnp.mean(widened * widened, axis=1, keepdims=True) + 1e-06)
        return (scaled, factor)

    gate_pieces = pieces_of(ffn_gate_w, 1)
    up_pieces = pieces_of(ffn_up_w, 1)
    down_pieces = pieces_of(ffn_down_w, 0)

    def feed_forward(values, gain):
        scaled, factor = norm_rows(values, gain)
        inputs = [
            lax.dynamic_slice_in_dim(scaled, (z - s) % n_fs * block, block, 1) for s in range(n_fs)
        ]

        def project(gathered, k):
            total = None
            for s in range(n_fs):
                product = jnp.dot(inputs[s], gathered[s][k], preferred_element_type=jnp.float32)
                total = product if total is None else total + product
            return total

        hidden = [
            (
                jax.nn.silu(factor * project(gate_pieces, k)) * (factor * project(up_pieces, k))
            ).astype(jnp.bfloat16)
            for k in range(n_grp)
        ]
        out = jnp.zeros((rows, width), jnp.bfloat16)
        for s in range(n_fs):
            product = None
            for k in range(n_grp):
                term = jnp.dot(hidden[k], down_pieces[s][k], preferred_element_type=jnp.float32)
                product = term if product is None else product + term
            out = lax.dynamic_update_slice(
                out, product.astype(jnp.bfloat16), (0, (z - s) % n_fs * block)
            )
        return scatter_tp(out)

    first = (layer_input.astype(jnp.float32) + 0.5 * feed_forward(layer_input, first_gain)).astype(
        jnp.bfloat16
    )
    pool_in = absolute(pool_in_w, 0, 0)
    mixer_gate = absolute(mixer_gate_w, 0, 0)
    mixer_out = absolute(mixer_out_w, 1, 0)
    scaled, factor = norm_rows(first, mixer_gain)
    pool_pre = (factor * jnp.dot(scaled, pool_in, preferred_element_type=jnp.float32)).astype(
        jnp.bfloat16
    )
    gate_logit = factor * jnp.dot(scaled, mixer_gate, preferred_element_type=jnp.float32)
    groups, group_width = group_mix_w.shape[:2]
    position = lax.broadcasted_iota(jnp.int32, (rows, rows), 0)
    back = position - lax.broadcasted_iota(jnp.int32, (rows, rows), 1)
    row = lax.broadcasted_iota(jnp.int32, (rows, 1), 0)
    pooled = []
    for g in range(groups):
        window = 2 ** (1 + (t * groups + g) % 4)
        band = ((back >= 0) & (back < window)).astype(jnp.bfloat16)
        values = pool_pre[:, g * group_width : (g + 1) * group_width]
        sums = jnp.dot(band, values, preferred_element_type=jnp.float32)
        count = jnp.minimum(row + 1, window).astype(jnp.float32)
        trail = (sums / count - values.astype(jnp.float32)).astype(jnp.bfloat16)
        mixed = jnp.dot(trail, group_mix_w[g], preferred_element_type=jnp.float32)
        pooled.append(mixed)
    pooled = (jnp.concatenate(pooled, axis=1) * pool_scale).astype(jnp.bfloat16)
    lifted = scatter_tp(
        jnp.dot(pooled, mixer_out, preferred_element_type=jnp.float32).astype(jnp.bfloat16)
    )
    second = (first.astype(jnp.float32) + jax.nn.sigmoid(gate_logit) * lifted).astype(jnp.bfloat16)
    result = second.astype(jnp.float32) + 0.5 * feed_forward(second, second_gain)
    return result.astype(jnp.bfloat16)


def solution(mesh):
    return jax.shard_map(
        per_device,
        mesh=mesh,
        in_specs=(
            P(("grp", "fs"), "tp"),
            P(None, "tp"),
            P("fs", "tp"),
            P("fs", "tp"),
            P("tp", "fs"),
            P(None, "tp"),
            P("fs", "tp"),
            P("fs", "tp"),
            P("tp", None, None),
            P(None, "tp"),
            P("tp", "fs"),
            P(None, "tp"),
        ),
        out_specs=P(("grp", "fs"), "tp"),
        check_vma=False,
    )
```

profile of v0, /device:TPU:0, one launch (start us, length us, event | category | flops | bytes accessed | tf_op | source)
XLA Modules:
  0.0 356.5 jit_solution(13257093705416114040)
XLA Ops:
  0.0 3.0 collective-permute-start.1
  4.3 1.6 collective-permute-start.3
  6.0 1.6 collective-permute-start.6
  7.6 4.8 %collective-permute-done.1 = bf16[384,512]{1,0:T(8,128)(2,1)} collective-permute-done((bf16[384,512]{1,0:T(8,128)(2,1)}, bf16[384,512]{1,0:T(8,128)(2,1)}, u32[]{:S(2)}, u32[]{:S(2)}) %collective-permute-start.1) | collective-permute-done | bytes 393248 | tf_op jit(solution)/shard_map/ppermute | solution.py:67
  13.4 1.8 collective-permute-start.15
  15.2 5.2 %all_gather.9 = bf16[1,2048]{1,0:T(2,128)(2,1)S(1)} all-gather(bf16[1,512]{1,0:T(2,128)(2,1)S(1)} %copy-done.40), channel_id=1, replica_groups=mesh['grp'=2,'fs'=4,'tp'=4] {'tp'}, dimensions={1}, use_global_device_ids=true | all-gather | bytes 5120 | tf_op jit(solution)/shard_map/all_gather | solution.py:95
  22.9 3.8 %collective-permute-done.3 = bf16[512,768]{1,0:T(8,128)(2,1)} collective-permute-done((bf16[512,768]{1,0:T(8,128)(2,1)S(1)}, bf16[512,768]{1,0:T(8,128)(2,1)}, u32[]{:S(2)}, u32[]{:S(2)}) %collective-permute-start.3) | collective-permute-done | bytes 786464 | tf_op jit(solution)/shard_map/ppermute | solution.py:45
  26.7 1.5 collective-permute-start.9
  30.8 12.8 %collective-permute-done.6 = bf16[512,768]{1,0:T(8,128)(2,1)} collective-permute-done((bf16[512,768]{1,0:T(8,128)(2,1)S(1)}, bf16[512,768]{1,0:T(8,128)(2,1)}, u32[]{:S(2)}, u32[]{:S(2)}) %collective-permute-start.6) | collective-permute-done | bytes 786464 | tf_op jit(solution)/shard_map/ppermute | solution.py:45
  43.5 1.6 fusion.128
  45.6 1.7 fusion.126
  47.9 1.6 collective-permute-start.12
  49.4 10.9 %collective-permute-done.15 = bf16[768,512]{1,0:T(8,128)(2,1)} collective-permute-done((bf16[768,512]{1,0:T(8,128)(2,1)}, bf16[768,512]{1,0:T(8,128)(2,1)}, u32[]{:S(2)}, u32[]{:S(2)}) %collective-permute-start.15) | collective-permute-done | bytes 786464 | tf_op jit(solution)/shard_map/ppermute | solution.py:45
  60.4 1.5 collective-permute-start.16
  62.0 15.1 %collective-permute-done.4 = bf16[512,768]{1,0:T(8,128)(2,1)S(1)} collective-permute-done((bf16[512,768]{1,0:T(8,128)(2,1)}, bf16[512,768]{1,0:T(8,128)(2,1)S(1)}, u32[]{:S(2)}, u32[]{:S(2)}) %collective-permute-start.4) | collective-permute-done | bytes 786464 | tf_op jit(solution)/shard_map/ppermute | solution.py:45
  79.6 14.4 %collective-permute-done.7 = bf16[512,768]{1,0:T(8,128)(2,1)S(1)} collective-permute-done((bf16[512,768]{1,0:T(8,128)(2,1)}, bf16[512,768]{1,0:T(8,128)(2,1)S(1)}, u32[]{:S(2)}, u32[]{:S(2)}) %collective-permute-start.7) | collective-permute-done | bytes 786464 | tf_op jit(solution)/shard_map/ppermute | solution.py:45
  96.3 14.5 %collective-permute-done.17 = bf16[768,512]{1,0:T(8,128)(2,1)S(1)} collective-permute-done((bf16[768,512]{1,0:T(8,128)(2,1)}, bf16[768,512]{1,0:T(8,128)(2,1)S(1)}, u32[]{:S(2)}, u32[]{:S(2)}) %collective-permute-start.17) | collective-permute-done | bytes 786464 | tf_op jit(solution)/shard_map/ppermute | solution.py:45
  110.8 1.5 collective-permute-start.13
  113.5 14.2 %collective-permute-done.5 = bf16[512,768]{1,0:T(8,128)(2,1)S(1)} collective-permute-done((bf16[512,768]{1,0:T(8,128)(2,1)S(1)}, bf16[512,768]{1,0:T(8,128)(2,1)S(1)}, u32[]{:S(2)}, u32[]{:S(2)}) %collective-permute-start.5) | collective-permute-done | bytes 786464 | tf_op jit(solution)/shard_map/ppermute | solution.py:45
  128.2 16.3 %collective-permute-done.8 = bf16[512,768]{1,0:T(8,128)(2,1)S(1)} collective-permute-done((bf16[512,768]{1,0:T(8,128)(2,1)S(1)}, bf16[512,768]{1,0:T(8,128)(2,1)S(1)}, u32[]{:S(2)}, u32[]{:S(2)}) %collective-permute-start.8) | collective-permute-done | bytes 786464 | tf_op jit(solution)/shard_map/ppermute | solution.py:45
  144.5 1.5 collective-permute-start.11
  146.7 1.6 fusion.198
  148.3 1.6 fusion.199
  150.4 9.6 %collective-permute-done.19 = bf16[768,512]{1,0:T(8,128)(2,1)S(1)} collective-permute-done((bf16[768,512]{1,0:T(8,128)(2,1)S(1)}, bf16[768,512]{1,0:T(8,128)(2,1)S(1)}, u32[]{:S(2)}, u32[]{:S(2)}) %collective-permute-start.19) | collective-permute-done | bytes 786464 | tf_op jit(solution)/shard_map/ppermute | solution.py:45
  160.0 1.5 collective-permute-start.14
  164.0 16.4 %collective-permute-done.14 = bf16[512,768]{1,0:T(8,128)(2,1)S(1)} collective-permute-done((bf16[512,768]{1,0:T(8,128)(2,1)S(1)}, bf16[512,768]{1,0:T(8,128)(2,1)S(1)}, u32[]{:S(2)}, u32[]{:S(2)}) %collective-permute-start.14) | collective-permute-done | bytes 786464 | tf_op jit(solution)/shard_map/ppermute | solution.py:47
  183.0 12.1 %collective-permute-done.20 = bf16[768,512]{1,0:T(8,128)(2,1)S(1)} collective-permute-done((bf16[768,512]{1,0:T(8,128)(2,1)S(1)}, bf16[768,512]{1,0:T(8,128)(2,1)S(1)}, u32[]{:S(2)}, u32[]{:S(2)}) %collective-permute-start.20) | collective-permute-done | bytes 786464 | tf_op jit(solution)/shard_map/ppermute | solution.py:47
  198.7 1.6 constant_dynamic-update-slice_fusion.10
  201.5 1.6 constant_dynamic-slice_fusion.3
  206.6 1.6 collective-permute-start.27
  208.2 2.0 add_convert_fusion.4
  210.8 1.6 dynamic-slice_dynamic-update-slice_fusion.1
  212.4 10.5 %all_gather.10 = bf16[1,2048]{1,0:T(2,128)(2,1)S(1)} all-gather(bf16[1,512]{1,0:T(2,128)(2,1)S(1)} %copy-done.41), channel_id=1, replica_groups=mesh['grp'=2,'fs'=4,'tp'=4] {'tp'}, dimensions={1}, use_global_device_ids=true | all-gather | bytes 5120 | tf_op jit(solution)/shard_map/all_gather | solution.py:95
  223.0 1.6 dynamic-slice_dynamic-update-slice_fusion.2
  224.6 1.5 collective-permute-start.34
  226.1 2.1 collective-permute-start.35
  231.4 1.6 constant_dynamic-update-slice_fusion.9
  233.0 2.9 dynamic_update_slice.162
  235.8 1.5 collective-permute-start.36
  237.3 2.3 collective-permute-start.37
  241.0 2.0 dynamic_update_slice.163
  243.0 3.4 dynamic_update_slice.164
  250.9 1.9 collective-permute-done.42
  252.8 1.7 collective-permute-start.29
  254.5 2.1 dynamic_update_slice.165
  256.6 3.4 dynamic_update_slice.166
  259.9 2.1 dynamic_update_slice.167
  264.0 2.5 fusion.61
  269.2 1.9 convolution_convert_fusion
  271.3 3.4 collective-permute-start.28
  275.4 1.7 constant_dynamic-update-slice_fusion.16
  277.1 4.9 %collective-permute-done.28 = bf16[256,512]{1,0:T(8,128)(2,1)S(1)} collective-permute-done((bf16[256,512]{1,0:T(8,128)(2,1)}, bf16[256,512]{1,0:T(8,128)(2,1)S(1)}, u32[]{:S(2)}, u32[]{:S(2)}) %collective-permute-start.28) | collective-permute-done | bytes 262176 | tf_op jit(solution)/shard_map/ppermute | solution.py:47
  282.7 2.3 collective-permute-done.31
  286.7 1.7 constant_dynamic-update-slice_fusion.14
  289.9 3.1 collective-permute-done.32
  293.7 3.3 collective-permute-done.46
  297.3 2.8 constant_dynamic-update-slice_fusion.3
  301.4 9.4 %collective-permute-done.49 = bf16[384,512]{1,0:T(8,128)(2,1)S(1)} collective-permute-done((bf16[384,512]{1,0:T(8,128)(2,1)S(1)}, bf16[384,512]{1,0:T(8,128)(2,1)S(1)}, u32[]{:S(2)}, u32[]{:S(2)}) %collective-permute-start.49) | collective-permute-done | bytes 393248 | tf_op jit(solution)/shard_map/ppermute | solution.py:67
  310.8 5.4 %all_gather.11 = bf16[1,2048]{1,0:T(2,128)(2,1)S(1)} all-gather(bf16[1,512]{1,0:T(2,128)(2,1)S(1)} %copy-done.42), channel_id=1, replica_groups=mesh['grp'=2,'fs'=4,'tp'=4] {'tp'}, dimensions={1}, use_global_device_ids=true | all-gather | bytes 5120 | tf_op jit(solution)/shard_map/all_gather | solution.py:95
  320.0 1.7 fusion.104
  323.3 1.7 fusion.102
  326.8 1.7 fusion.202
  335.4 1.7 fusion.203
  345.4 10.1 %collective-permute-done.52 = bf16[384,512]{1,0:T(8,128)(2,1)S(1)} collective-permute-done((bf16[384,512]{1,0:T(8,128)(2,1)S(1)}, bf16[384,512]{1,0:T(8,128)(2,1)S(1)}, u32[]{:S(2)}, u32[]{:S(2)}) %collective-permute-start.52) | collective-permute-done | bytes 393248 | tf_op jit(solution)/shard_map/ppermute | solution.py:87
  (264 shorter events, 73.3 us)
Async XLA Ops:
  0.0 12.4 %collective-permute-start.1 = (bf16[384,512]{1,0:T(8,128)(2,1)}, bf16[384,512]{1,0:T(8,128)(2,1)}, u32[]{:S(2)}, u32[]{:S(2)}) collective-permute-start(bf16[384,512]{1,0:T(8,128)(2,1)} %param.12), channel_id=1, source_target_pairs={{0,2},{1,3},{2,0},{3,1},{4,6},{5,7},{6,4},{7,5},{8,10},{9,11},{10,... | collective-permute-start | bytes 1179656 | tf_op jit(solution)/shard_map/ppermute | solution.py:67
  4.3 22.4 %collective-permute-start.3 = (bf16[512,768]{1,0:T(8,128)(2,1)S(1)}, bf16[512,768]{1,0:T(8,128)(2,1)}, u32[]{:S(2)}, u32[]{:S(2)}) collective-permute-start(bf16[512,768]{1,0:T(8,128)(2,1)S(1)} %constant_dynamic-slice_fusion.11), channel_id=1, source_target_pairs={{0,4},{4,8},{8,12},{12,0},{1,5},{5,9},{9,13},{13,1},{2,6},{6,10},{... | collective-permute-start | bytes 2359304 | tf_op jit(solution)/shard_map/ppermute | solution.py:45
  5.9 14.8 %collective-permute-start = (bf16[384,512]{1,0:T(8,128)(2,1)}, bf16[384,512]{1,0:T(8,128)(2,1)}, u32[]{:S(2)}, u32[]{:S(2)}) collective-permute-start(bf16[384,512]{1,0:T(8,128)(2,1)} %param.12), channel_id=1, source_target_pairs={{0,1},{1,0},{2,3},{3,2},{4,5},{5,4},{6,7},{7,6},{8,9},{9,8},{10,11... | collective-permute-start | bytes 1179656 | tf_op jit(solution)/shard_map/ppermute | solution.py:65
  6.0 14.7 %copy-start.35 = (bf16[384,512]{1,0:T(8,128)(2,1)S(1)}, bf16[384,512]{1,0:T(8,128)(2,1)}, u32[]{:S(2)}) copy-start(bf16[384,512]{1,0:T(8,128)(2,1)} %param.12) | copy-start | bytes 1179652
  6.0 37.5 %collective-permute-start.6 = (bf16[512,768]{1,0:T(8,128)(2,1)S(1)}, bf16[512,768]{1,0:T(8,128)(2,1)}, u32[]{:S(2)}, u32[]{:S(2)}) collective-permute-start(bf16[512,768]{1,0:T(8,128)(2,1)S(1)} %constant_dynamic-slice_fusion.10), channel_id=1, source_target_pairs={{0,4},{4,8},{8,12},{12,0},{1,5},{5,9},{9,13},{13,1},{2,6},{6,10},{... | collective-permute-start | bytes 2359304 | tf_op jit(solution)/shard_map/ppermute | solution.py:45
  12.4 15.8 %collective-permute-start.2 = (bf16[384,512]{1,0:T(8,128)(2,1)}, bf16[384,512]{1,0:T(8,128)(2,1)}, u32[]{:S(2)}, u32[]{:S(2)}) collective-permute-start(bf16[384,512]{1,0:T(8,128)(2,1)} %collective-permute-done.1), channel_id=1, source_target_pairs={{0,1},{1,0},{2,3},{3,2},{4,5},{5,4},{6,7},{7,6},{8,9},{9,8},{10,11... | collective-permute-start | bytes 1179656 | tf_op jit(solution)/shard_map/ppermute | solution.py:70
  13.4 47.0 %collective-permute-start.15 = (bf16[768,512]{1,0:T(8,128)(2,1)}, bf16[768,512]{1,0:T(8,128)(2,1)}, u32[]{:S(2)}, u32[]{:S(2)}) collective-permute-start(bf16[768,512]{1,0:T(8,128)(2,1)} %constant_dynamic-slice_fusion.9), channel_id=1, source_target_pairs={{0,4},{4,8},{8,12},{12,0},{1,5},{5,9},{9,13},{13,1},{2,6},{6,10},{... | collective-permute-start | bytes 2359304 | tf_op jit(solution)/shard_map/ppermute | solution.py:45
  26.7 35.2 %collective-permute-start.9 = (bf16[512,768]{1,0:T(8,128)(2,1)}, bf16[512,768]{1,0:T(8,128)(2,1)S(1)}, u32[]{:S(2)}, u32[]{:S(2)}) collective-permute-start(bf16[512,768]{1,0:T(8,128)(2,1)} %collective-permute-done.3), channel_id=1, source_target_pairs={{0,16},{16,0},{1,17},{17,1},{2,18},{18,2},{3,19},{19,3},{4,20},{20... | collective-permute-start | bytes 2359304 | tf_op jit(solution)/shard_map/ppermute | solution.py:47
  28.2 48.9 %collective-permute-start.4 = (bf16[512,768]{1,0:T(8,128)(2,1)}, bf16[512,768]{1,0:T(8,128)(2,1)S(1)}, u32[]{:S(2)}, u32[]{:S(2)}) collective-permute-start(bf16[512,768]{1,0:T(8,128)(2,1)} %collective-permute-done.3), channel_id=1, source_target_pairs={{0,4},{4,8},{8,12},{12,0},{1,5},{5,9},{9,13},{13,1},{2,6},{6,10},{... | collective-permute-start | bytes 2359304 | tf_op jit(solution)/shard_map/ppermute | solution.py:45
  30.7 14.4 %copy-start.7 = (bf16[512,1536]{1,0:T(8,128)(2,1)S(1)}, bf16[512,1536]{1,0:T(8,128)(2,1)}, u32[]{:S(2)}) copy-start(bf16[512,1536]{1,0:T(8,128)(2,1)} %param.14) | copy-start | bytes 4718596
  43.5 50.5 %collective-permute-start.7 = (bf16[512,768]{1,0:T(8,128)(2,1)}, bf16[512,768]{1,0:T(8,128)(2,1)S(1)}, u32[]{:S(2)}, u32[]{:S(2)}) collective-permute-start(bf16[512,768]{1,0:T(8,128)(2,1)} %collective-permute-done.6), channel_id=1, source_target_pairs={{0,4},{4,8},{8,12},{12,0},{1,5},{5,9},{9,13},{13,1},{2,6},{6,10},{... | collective-permute-start | bytes 2359304 | tf_op jit(solution)/shard_map/ppermute | solution.py:45
  47.9 46.6 %collective-permute-start.12 = (bf16[512,768]{1,0:T(8,128)(2,1)}, bf16[512,768]{1,0:T(8,128)(2,1)S(1)}, u32[]{:S(2)}, u32[]{:S(2)}) collective-permute-start(bf16[512,768]{1,0:T(8,128)(2,1)} %collective-permute-done.6), channel_id=1, source_target_pairs={{0,16},{16,0},{1,17},{17,1},{2,18},{18,2},{3,19},{19,3},{4,20},{20... | collective-permute-start | bytes 2359304 | tf_op jit(solution)/shard_map/ppermute | solution.py:47
  60.4 121.7 %collective-permute-start.16 = (bf16[768,512]{1,0:T(8,128)(2,1)}, bf16[768,512]{1,0:T(8,128)(2,1)S(1)}, u32[]{:S(2)}, u32[]{:S(2)}) collective-permute-start(bf16[768,512]{1,0:T(8,128)(2,1)} %collective-permute-done.15), channel_id=1, source_target_pairs={{0,16},{16,0},{1,17},{17,1},{2,18},{18,2},{3,19},{19,3},{4,20},{20... | collective-permute-start | bytes 2359304 | tf_op jit(solution)/shard_map/ppermute | solution.py:47
  61.9 17.7 %copy-start.9 = (bf16[512,768]{1,0:T(8,128)(2,1)}, bf16[512,768]{1,0:T(8,128)(2,1)S(1)}, u32[]{:S(2)}) copy-start(bf16[512,768]{1,0:T(8,128)(2,1)S(1)} %collective-permute-done.9) | copy-start | bytes 2359300
  61.9 48.9 %collective-permute-start.17 = (bf16[768,512]{1,0:T(8,128)(2,1)}, bf16[768,512]{1,0:T(8,128)(2,1)S(1)}, u32[]{:S(2)}, u32[]{:S(2)}) collective-permute-start(bf16[768,512]{1,0:T(8,128)(2,1)} %collective-permute-done.15), channel_id=1, source_target_pairs={{0,4},{4,8},{8,12},{12,0},{1,5},{5,9},{9,13},{13,1},{2,6},{6,10},{... | collective-permute-start | bytes 2359304 | tf_op jit(solution)/shard_map/ppermute | solution.py:45
  77.1 16.9 %copy-start.11 = (bf16[512,768]{1,0:T(8,128)(2,1)}, bf16[512,768]{1,0:T(8,128)(2,1)S(1)}, u32[]{:S(2)}) copy-start(bf16[512,768]{1,0:T(8,128)(2,1)S(1)} %collective-permute-done.4) | copy-start | bytes 2359300
  77.1 35.2 %collective-permute-start.10 = (bf16[512,768]{1,0:T(8,128)(2,1)S(1)}, bf16[512,768]{1,0:T(8,128)(2,1)S(1)}, u32[]{:S(2)}, u32[]{:S(2)}) collective-permute-start(bf16[512,768]{1,0:T(8,128)(2,1)S(1)} %collective-permute-done.4), channel_id=1, source_target_pairs={{0,16},{16,0},{1,17},{17,1},{2,18},{18,2},{3,19},{19,3},{4,20},{20... | collective-permute-start | bytes 2359304 | tf_op jit(solution)/shard_map/ppermute | solution.py:47
  94.0 16.9 %copy-start.15 = (bf16[512,768]{1,0:T(8,128)(2,1)}, bf16[512,768]{1,0:T(8,128)(2,1)S(1)}, u32[]{:S(2)}) copy-start(bf16[512,768]{1,0:T(8,128)(2,1)S(1)} %collective-permute-done.7) | copy-start | bytes 2359300
  94.0 33.7 %collective-permute-start.5 = (bf16[512,768]{1,0:T(8,128)(2,1)S(1)}, bf16[512,768]{1,0:T(8,128)(2,1)S(1)}, u32[]{:S(2)}, u32[]{:S(2)}) collective-permute-start(bf16[512,768]{1,0:T(8,128)(2,1)S(1)} %collective-permute-done.4), channel_id=1, source_target_pairs={{0,4},{4,8},{8,12},{12,0},{1,5},{5,9},{9,13},{13,1},{2,6},{6,10},{... | collective-permute-start | bytes 2359304 | tf_op jit(solution)/shard_map/ppermute | solution.py:45
  94.5 17.9 %copy-start.13 = (bf16[512,768]{1,0:T(8,128)(2,1)}, bf16[512,768]{1,0:T(8,128)(2,1)S(1)}, u32[]{:S(2)}) copy-start(bf16[512,768]{1,0:T(8,128)(2,1)S(1)} %collective-permute-done.12) | copy-start | bytes 2359300
  94.5 50.1 %collective-permute-start.8 = (bf16[512,768]{1,0:T(8,128)(2,1)S(1)}, bf16[512,768]{1,0:T(8,128)(2,1)S(1)}, u32[]{:S(2)}, u32[]{:S(2)}) collective-permute-start(bf16[512,768]{1,0:T(8,128)(2,1)S(1)} %collective-permute-done.7), channel_id=1, source_target_pairs={{0,4},{4,8},{8,12},{12,0},{1,5},{5,9},{9,13},{13,1},{2,6},{6,10},{... | collective-permute-start | bytes 2359304 | tf_op jit(solution)/shard_map/ppermute | solution.py:45
  110.8 39.1 %copy-start.23 = (bf16[768,512]{1,0:T(8,128)(2,1)}, bf16[768,512]{1,0:T(8,128)(2,1)S(1)}, u32[]{:S(2)}) copy-start(bf16[768,512]{1,0:T(8,128)(2,1)S(1)} %collective-permute-done.17) | copy-start | bytes 2359300
  110.8 51.2 %collective-permute-start.13 = (bf16[512,768]{1,0:T(8,128)(2,1)S(1)}, bf16[512,768]{1,0:T(8,128)(2,1)S(1)}, u32[]{:S(2)}, u32[]{:S(2)}) collective-permute-start(bf16[512,768]{1,0:T(8,128)(2,1)S(1)} %collective-permute-done.7), channel_id=1, source_target_pairs={{0,16},{16,0},{1,17},{17,1},{2,18},{18,2},{3,19},{19,3},{4,20},{20... | collective-permute-start | bytes 2359304 | tf_op jit(solution)/shard_map/ppermute | solution.py:47
  112.4 70.2 %collective-permute-start.18 = (bf16[768,512]{1,0:T(8,128)(2,1)S(1)}, bf16[768,512]{1,0:T(8,128)(2,1)S(1)}, u32[]{:S(2)}, u32[]{:S(2)}) collective-permute-start(bf16[768,512]{1,0:T(8,128)(2,1)S(1)} %collective-permute-done.17), channel_id=1, source_target_pairs={{0,16},{16,0},{1,17},{17,1},{2,18},{18,2},{3,19},{19,3},{4,20},{20... | collective-permute-start | bytes 2359304 | tf_op jit(solution)/shard_map/ppermute | solution.py:47
  127.7 16.9 %copy-start.33 = (bf16[512,768]{1,0:T(8,128)(2,1)}, bf16[512,768]{1,0:T(8,128)(2,1)S(1)}, u32[]{:S(2)}) copy-start(bf16[512,768]{1,0:T(8,128)(2,1)S(1)} %collective-permute-done.5) | copy-start | bytes 2359300
  127.7 32.4 %collective-permute-start.19 = (bf16[768,512]{1,0:T(8,128)(2,1)S(1)}, bf16[768,512]{1,0:T(8,128)(2,1)S(1)}, u32[]{:S(2)}, u32[]{:S(2)}) collective-permute-start(bf16[768,512]{1,0:T(8,128)(2,1)S(1)} %collective-permute-done.17), channel_id=1, source_target_pairs={{0,4},{4,8},{8,12},{12,0},{1,5},{5,9},{9,13},{13,1},{2,6},{6,10},{... | collective-permute-start | bytes 2359304 | tf_op jit(solution)/shard_map/ppermute | solution.py:45
  144.5 15.5 %copy-start.45 = (bf16[512,768]{1,0:T(8,128)(2,1)}, bf16[512,768]{1,0:T(8,128)(2,1)S(1)}, u32[]{:S(2)}) copy-start(bf16[512,768]{1,0:T(8,128)(2,1)S(1)} %collective-permute-done.8) | copy-start | bytes 2359300
  144.5 18.6 %collective-permute-start.11 = (bf16[512,768]{1,0:T(8,128)(2,1)S(1)}, bf16[512,768]{1,0:T(8,128)(2,1)S(1)}, u32[]{:S(2)}, u32[]{:S(2)}) collective-permute-start(bf16[512,768]{1,0:T(8,128)(2,1)S(1)} %collective-permute-done.5), channel_id=1, source_target_pairs={{0,16},{16,0},{1,17},{17,1},{2,18},{18,2},{3,19},{19,3},{4,20},{20... | collective-permute-start | bytes 2359304 | tf_op jit(solution)/shard_map/ppermute | solution.py:47
  160.0 20.4 %collective-permute-start.14 = (bf16[512,768]{1,0:T(8,128)(2,1)S(1)}, bf16[512,768]{1,0:T(8,128)(2,1)S(1)}, u32[]{:S(2)}, u32[]{:S(2)}) collective-permute-start(bf16[512,768]{1,0:T(8,128)(2,1)S(1)} %collective-permute-done.8), channel_id=1, source_target_pairs={{0,16},{16,0},{1,17},{17,1},{2,18},{18,2},{3,19},{19,3},{4,20},{20... | collective-permute-start | bytes 2359304 | tf_op jit(solution)/shard_map/ppermute | solution.py:47
  162.0 33.1 %collective-permute-start.20 = (bf16[768,512]{1,0:T(8,128)(2,1)S(1)}, bf16[768,512]{1,0:T(8,128)(2,1)S(1)}, u32[]{:S(2)}, u32[]{:S(2)}) collective-permute-start(bf16[768,512]{1,0:T(8,128)(2,1)S(1)} %collective-permute-done.19), channel_id=1, source_target_pairs={{0,16},{16,0},{1,17},{17,1},{2,18},{18,2},{3,19},{19,3},{4,20},{20... | collective-permute-start | bytes 2359304 | tf_op jit(solution)/shard_map/ppermute | solution.py:47
  197.7 10.6 %collective-permute-start.21 = (bf16[384,512]{1,0:T(8,128)(2,1)}, bf16[384,512]{1,0:T(8,128)(2,1)}, u32[]{:S(2)}, u32[]{:S(2)}) collective-permute-start(bf16[384,512]{1,0:T(8,128)(2,1)} %get-tuple-element.17), channel_id=1, source_target_pairs={{0,1},{1,0},{2,3},{3,2},{4,5},{5,4},{6,7},{7,6},{8,9},{9,8},{10,11... | collective-permute-start | bytes 1179656 | tf_op jit(solution)/shard_map/ppermute | solution.py:84
  200.4 24.2 %collective-permute-start.33 = (bf16[256,256]{1,0:T(8,128)(2,1)}, bf16[256,256]{1,0:T(8,128)(2,1)}, u32[]{:S(2)}, u32[]{:S(2)}) collective-permute-start(bf16[256,256]{1,0:T(8,128)(2,1)} %get-tuple-element.6), channel_id=1, source_target_pairs={{0,4},{4,8},{8,12},{12,0},{1,5},{5,9},{9,13},{13,1},{2,6},{6,10},{... | collective-permute-start | bytes 393224 | tf_op jit(solution)/shard_map/ppermute | solution.py:45
  203.1 23.0 %collective-permute-start.39 = (bf16[128,512]{1,0:T(8,128)(2,1)}, bf16[128,512]{1,0:T(8,128)(2,1)}, u32[]{:S(2)}, u32[]{:S(2)}) collective-permute-start(bf16[128,512]{1,0:T(8,128)(2,1)} %get-tuple-element.21), channel_id=1, source_target_pairs={{0,4},{4,8},{8,12},{12,0},{1,5},{5,9},{9,13},{13,1},{2,6},{6,10},{... | collective-permute-start | bytes 393224 | tf_op jit(solution)/shard_map/ppermute | solution.py:45
  206.6 33.7 %collective-permute-start.27 = (bf16[256,512]{1,0:T(8,128)(2,1)}, bf16[256,512]{1,0:T(8,128)(2,1)}, u32[]{:S(2)}, u32[]{:S(2)}) collective-permute-start(bf16[256,512]{1,0:T(8,128)(2,1)} %get-tuple-element.10), channel_id=1, source_target_pairs={{0,4},{4,8},{8,12},{12,0},{1,5},{5,9},{9,13},{13,1},{2,6},{6,10},{... | collective-permute-start | bytes 786440 | tf_op jit(solution)/shard_map/ppermute | solution.py:45
  208.2 20.0 %collective-permute-start.23 = (bf16[384,512]{1,0:T(8,128)(2,1)}, bf16[384,512]{1,0:T(8,128)(2,1)}, u32[]{:S(2)}, u32[]{:S(2)}) collective-permute-start(bf16[384,512]{1,0:T(8,128)(2,1)} %get-tuple-element.18), channel_id=1, source_target_pairs={{0,1},{1,0},{2,3},{3,2},{4,5},{5,4},{6,7},{7,6},{8,9},{9,8},{10,11... | collective-permute-start | bytes 1179656 | tf_op jit(solution)/shard_map/ppermute | solution.py:84
  210.2 18.6 %collective-permute-start.22 = (bf16[384,512]{1,0:T(8,128)(2,1)}, bf16[384,512]{1,0:T(8,128)(2,1)}, u32[]{:S(2)}, u32[]{:S(2)}) collective-permute-start(bf16[384,512]{1,0:T(8,128)(2,1)} %add_convert_fusion.4), channel_id=1, source_target_pairs={{0,2},{1,3},{2,0},{3,1},{4,6},{5,7},{6,4},{7,5},{8,10},{9,11},{10,... | collective-permute-start | bytes 1179656 | tf_op jit(solution)/shard_map/ppermute | solution.py:87
  224.6 6.0 %collective-permute-start.34 = (bf16[256,256]{1,0:T(8,128)(2,1)}, bf16[256,256]{1,0:T(8,128)(2,1)S(1)}, u32[]{:S(2)}, u32[]{:S(2)}) collective-permute-start(bf16[256,256]{1,0:T(8,128)(2,1)} %collective-permute-done.33), channel_id=1, source_target_pairs={{0,16},{16,0},{1,17},{17,1},{2,18},{18,2},{3,19},{19,3},{4,20},{20... | collective-permute-start | bytes 393224 | tf_op jit(solution)/shard_map/ppermute | solution.py:47
  226.1 9.7 %collective-permute-start.35 = (bf16[256,256]{1,0:T(8,128)(2,1)}, bf16[256,256]{1,0:T(8,128)(2,1)S(1)}, u32[]{:S(2)}, u32[]{:S(2)}) collective-permute-start(bf16[256,256]{1,0:T(8,128)(2,1)} %collective-permute-done.33), channel_id=1, source_target_pairs={{0,4},{4,8},{8,12},{12,0},{1,5},{5,9},{9,13},{13,1},{2,6},{6,10},{... | collective-permute-start | bytes 393224 | tf_op jit(solution)/shard_map/ppermute | solution.py:45
  228.2 9.1 %collective-permute-start.40 = (bf16[128,512]{1,0:T(8,128)(2,1)}, bf16[128,512]{1,0:T(8,128)(2,1)S(1)}, u32[]{:S(2)}, u32[]{:S(2)}) collective-permute-start(bf16[128,512]{1,0:T(8,128)(2,1)} %collective-permute-done.39), channel_id=1, source_target_pairs={{0,16},{16,0},{1,17},{17,1},{2,18},{18,2},{3,19},{19,3},{4,20},{20... | collective-permute-start | bytes 393224 | tf_op jit(solution)/shard_map/ppermute | solution.py:47
  228.7 10.9 %collective-permute-start.41 = (bf16[128,512]{1,0:T(8,128)(2,1)}, bf16[128,512]{1,0:T(8,128)(2,1)S(1)}, u32[]{:S(2)}, u32[]{:S(2)}) collective-permute-start(bf16[128,512]{1,0:T(8,128)(2,1)} %collective-permute-done.39), channel_id=1, source_target_pairs={{0,4},{4,8},{8,12},{12,0},{1,5},{5,9},{9,13},{13,1},{2,6},{6,10},{... | collective-permute-start | bytes 393224 | tf_op jit(solution)/shard_map/ppermute | solution.py:45
  230.5 32.2 %copy-start.38 = (bf16[384,512]{1,0:T(8,128)(2,1)}, bf16[384,512]{1,0:T(8,128)(2,1)S(1)}, u32[]{:S(2)}) copy-start(bf16[384,512]{1,0:T(8,128)(2,1)S(1)} %get-tuple-element.8) | copy-start | bytes 1179652
  230.5 19.7 %collective-permute-start.25 = (bf16[384,512]{1,0:T(8,128)(2,1)S(1)}, bf16[384,512]{1,0:T(8,128)(2,1)S(1)}, u32[]{:S(2)}, u32[]{:S(2)}) collective-permute-start(bf16[384,512]{1,0:T(8,128)(2,1)S(1)} %get-tuple-element.8), channel_id=1, source_target_pairs={{0,2},{1,3},{2,0},{3,1},{4,6},{5,7},{6,4},{7,5},{8,10},{9,11},{10,... | collective-permute-start | bytes 1179656 | tf_op jit(solution)/shard_map/ppermute | solution.py:67
  235.8 10.6 %collective-permute-start.36 = (bf16[256,256]{1,0:T(8,128)(2,1)S(1)}, bf16[256,256]{1,0:T(8,128)(2,1)S(1)}, u32[]{:S(2)}, u32[]{:S(2)}) collective-permute-start(bf16[256,256]{1,0:T(8,128)(2,1)S(1)} %collective-permute-done.35), channel_id=1, source_target_pairs={{0,16},{16,0},{1,17},{17,1},{2,18},{18,2},{3,19},{19,3},{4,20},{20... | collective-permute-start | bytes 393224 | tf_op jit(solution)/shard_map/ppermute | solution.py:47
  237.3 10.2 %collective-permute-start.37 = (bf16[256,256]{1,0:T(8,128)(2,1)S(1)}, bf16[256,256]{1,0:T(8,128)(2,1)S(1)}, u32[]{:S(2)}, u32[]{:S(2)}) collective-permute-start(bf16[256,256]{1,0:T(8,128)(2,1)S(1)} %collective-permute-done.35), channel_id=1, source_target_pairs={{0,4},{4,8},{8,12},{12,0},{1,5},{5,9},{9,13},{13,1},{2,6},{6,10},{... | collective-permute-start | bytes 393224 | tf_op jit(solution)/shard_map/ppermute | solution.py:45
  239.6 8.8 %collective-permute-start.43 = (bf16[128,512]{1,0:T(8,128)(2,1)S(1)}, bf16[128,512]{1,0:T(8,128)(2,1)S(1)}, u32[]{:S(2)}, u32[]{:S(2)}) collective-permute-start(bf16[128,512]{1,0:T(8,128)(2,1)S(1)} %collective-permute-done.41), channel_id=1, source_target_pairs={{0,4},{4,8},{8,12},{12,0},{1,5},{5,9},{9,13},{13,1},{2,6},{6,10},{... | collective-permute-start | bytes 393224 | tf_op jit(solution)/shard_map/ppermute | solution.py:45
  240.4 22.4 %collective-permute-start.24 = (bf16[384,512]{1,0:T(8,128)(2,1)S(1)}, bf16[384,512]{1,0:T(8,128)(2,1)S(1)}, u32[]{:S(2)}, u32[]{:S(2)}) collective-permute-start(bf16[384,512]{1,0:T(8,128)(2,1)S(1)} %get-tuple-element.8), channel_id=1, source_target_pairs={{0,1},{1,0},{2,3},{3,2},{4,5},{5,4},{6,7},{7,6},{8,9},{9,8},{10,11... | collective-permute-start | bytes 1179656 | tf_op jit(solution)/shard_map/ppermute | solution.py:65
  246.4 6.4 %collective-permute-start.42 = (bf16[128,512]{1,0:T(8,128)(2,1)S(1)}, bf16[128,512]{1,0:T(8,128)(2,1)S(1)}, u32[]{:S(2)}, u32[]{:S(2)}) collective-permute-start(bf16[128,512]{1,0:T(8,128)(2,1)S(1)} %collective-permute-done.41), channel_id=1, source_target_pairs={{0,16},{16,0},{1,17},{17,1},{2,18},{18,2},{3,19},{19,3},{4,20},{20... | collective-permute-start | bytes 393224 | tf_op jit(solution)/shard_map/ppermute | solution.py:47
  247.5 14.5 %collective-permute-start.38 = (bf16[256,256]{1,0:T(8,128)(2,1)S(1)}, bf16[256,256]{1,0:T(8,128)(2,1)S(1)}, u32[]{:S(2)}, u32[]{:S(2)}) collective-permute-start(bf16[256,256]{1,0:T(8,128)(2,1)S(1)} %collective-permute-done.37), channel_id=1, source_target_pairs={{0,16},{16,0},{1,17},{17,1},{2,18},{18,2},{3,19},{19,3},{4,20},{20... | collective-permute-start | bytes 393224 | tf_op jit(solution)/shard_map/ppermute | solution.py:47
  248.5 11.5 %collective-permute-start.44 = (bf16[128,512]{1,0:T(8,128)(2,1)S(1)}, bf16[128,512]{1,0:T(8,128)(2,1)S(1)}, u32[]{:S(2)}, u32[]{:S(2)}) collective-permute-start(bf16[128,512]{1,0:T(8,128)(2,1)S(1)} %collective-permute-done.43), channel_id=1, source_target_pairs={{0,16},{16,0},{1,17},{17,1},{2,18},{18,2},{3,19},{19,3},{4,20},{20... | collective-permute-start | bytes 393224 | tf_op jit(solution)/shard_map/ppermute | solution.py:47
  250.2 12.6 %collective-permute-start.26 = (bf16[384,512]{1,0:T(8,128)(2,1)S(1)}, bf16[384,512]{1,0:T(8,128)(2,1)S(1)}, u32[]{:S(2)}, u32[]{:S(2)}) collective-permute-start(bf16[384,512]{1,0:T(8,128)(2,1)S(1)} %collective-permute-done.25), channel_id=1, source_target_pairs={{0,1},{1,0},{2,3},{3,2},{4,5},{5,4},{6,7},{7,6},{8,9},{9,8},{10,11... | collective-permute-start | bytes 1179656 | tf_op jit(solution)/shard_map/ppermute | solution.py:70
  252.8 21.9 %collective-permute-start.29 = (bf16[256,512]{1,0:T(8,128)(2,1)}, bf16[256,512]{1,0:T(8,128)(2,1)}, u32[]{:S(2)}, u32[]{:S(2)}) collective-permute-start(bf16[256,512]{1,0:T(8,128)(2,1)} %collective-permute-done.27), channel_id=1, source_target_pairs={{0,4},{4,8},{8,12},{12,0},{1,5},{5,9},{9,13},{13,1},{2,6},{6,10},{... | collective-permute-start | bytes 786440 | tf_op jit(solution)/shard_map/ppermute | solution.py:45
  271.2 14.1 %collective-permute-start.45 = (bf16[384,512]{1,0:T(8,128)(2,1)S(1)}, bf16[384,512]{1,0:T(8,128)(2,1)S(1)}, u32[]{:S(2)}, u32[]{:S(2)}) collective-permute-start(bf16[384,512]{1,0:T(8,128)(2,1)S(1)} %get-tuple-element.15), channel_id=1, source_target_pairs={{0,1},{1,0},{2,3},{3,2},{4,5},{5,4},{6,7},{7,6},{8,9},{9,8},{10,11... | collective-permute-start | bytes 1179656 | tf_op jit(solution)/shard_map/ppermute | solution.py:84
  271.3 10.7 %collective-permute-start.28 = (bf16[256,512]{1,0:T(8,128)(2,1)}, bf16[256,512]{1,0:T(8,128)(2,1)S(1)}, u32[]{:S(2)}, u32[]{:S(2)}) collective-permute-start(bf16[256,512]{1,0:T(8,128)(2,1)} %collective-permute-done.27), channel_id=1, source_target_pairs={{0,16},{16,0},{1,17},{17,1},{2,18},{18,2},{3,19},{19,3},{4,20},{20... | collective-permute-start | bytes 786440 | tf_op jit(solution)/shard_map/ppermute | solution.py:47
  274.6 10.4 %collective-permute-start.31 = (bf16[256,512]{1,0:T(8,128)(2,1)}, bf16[256,512]{1,0:T(8,128)(2,1)S(1)}, u32[]{:S(2)}, u32[]{:S(2)}) collective-permute-start(bf16[256,512]{1,0:T(8,128)(2,1)} %collective-permute-done.29), channel_id=1, source_target_pairs={{0,4},{4,8},{8,12},{12,0},{1,5},{5,9},{9,13},{13,1},{2,6},{6,10},{... | collective-permute-start | bytes 786440 | tf_op jit(solution)/shard_map/ppermute | solution.py:45
  277.1 11.3 %collective-permute-start.30 = (bf16[256,512]{1,0:T(8,128)(2,1)}, bf16[256,512]{1,0:T(8,128)(2,1)S(1)}, u32[]{:S(2)}, u32[]{:S(2)}) collective-permute-start(bf16[256,512]{1,0:T(8,128)(2,1)} %collective-permute-done.29), channel_id=1, source_target_pairs={{0,16},{16,0},{1,17},{17,1},{2,18},{18,2},{3,19},{19,3},{4,20},{20... | collective-permute-start | bytes 786440 | tf_op jit(solution)/shard_map/ppermute | solution.py:47
  285.0 8.0 %collective-permute-start.32 = (bf16[256,512]{1,0:T(8,128)(2,1)S(1)}, bf16[256,512]{1,0:T(8,128)(2,1)S(1)}, u32[]{:S(2)}, u32[]{:S(2)}) collective-permute-start(bf16[256,512]{1,0:T(8,128)(2,1)S(1)} %collective-permute-done.31), channel_id=1, source_target_pairs={{0,16},{16,0},{1,17},{17,1},{2,18},{18,2},{3,19},{19,3},{4,20},{20... | collective-permute-start | bytes 786440 | tf_op jit(solution)/shard_map/ppermute | solution.py:47
  285.3 8.4 %collective-permute-start.47 = (bf16[384,512]{1,0:T(8,128)(2,1)S(1)}, bf16[384,512]{1,0:T(8,128)(2,1)S(1)}, u32[]{:S(2)}, u32[]{:S(2)}) collective-permute-start(bf16[384,512]{1,0:T(8,128)(2,1)S(1)} %get-tuple-element.16), channel_id=1, source_target_pairs={{0,1},{1,0},{2,3},{3,2},{4,5},{5,4},{6,7},{7,6},{8,9},{9,8},{10,11... | collective-permute-start | bytes 1179656 | tf_op jit(solution)/shard_map/ppermute | solution.py:84
  285.4 11.6 %collective-permute-start.46 = (bf16[384,512]{1,0:T(8,128)(2,1)S(1)}, bf16[384,512]{1,0:T(8,128)(2,1)S(1)}, u32[]{:S(2)}, u32[]{:S(2)}) collective-permute-start(bf16[384,512]{1,0:T(8,128)(2,1)S(1)} %add_convert_fusion.2), channel_id=1, source_target_pairs={{0,2},{1,3},{2,0},{3,1},{4,6},{5,7},{6,4},{7,5},{8,10},{9,11},{10,... | collective-permute-start | bytes 1179656 | tf_op jit(solution)/shard_map/ppermute | solution.py:87
  300.1 10.7 %collective-permute-start.49 = (bf16[384,512]{1,0:T(8,128)(2,1)S(1)}, bf16[384,512]{1,0:T(8,128)(2,1)S(1)}, u32[]{:S(2)}, u32[]{:S(2)}) collective-permute-start(bf16[384,512]{1,0:T(8,128)(2,1)S(1)} %get-tuple-element.24), channel_id=1, source_target_pairs={{0,2},{1,3},{2,0},{3,1},{4,6},{5,7},{6,4},{7,5},{8,10},{9,11},{10,... | collective-permute-start | bytes 1179656 | tf_op jit(solution)/shard_map/ppermute | solution.py:67
  301.4 14.9 %collective-permute-start.48 = (bf16[384,512]{1,0:T(8,128)(2,1)S(1)}, bf16[384,512]{1,0:T(8,128)(2,1)S(1)}, u32[]{:S(2)}, u32[]{:S(2)}) collective-permute-start(bf16[384,512]{1,0:T(8,128)(2,1)S(1)} %get-tuple-element.24), channel_id=1, source_target_pairs={{0,1},{1,0},{2,3},{3,2},{4,5},{5,4},{6,7},{7,6},{8,9},{9,8},{10,11... | collective-permute-start | bytes 1179656 | tf_op jit(solution)/shard_map/ppermute | solution.py:65
  310.8 5.6 %collective-permute-start.50 = (bf16[384,512]{1,0:T(8,128)(2,1)S(1)}, bf16[384,512]{1,0:T(8,128)(2,1)S(1)}, u32[]{:S(2)}, u32[]{:S(2)}) collective-permute-start(bf16[384,512]{1,0:T(8,128)(2,1)S(1)} %collective-permute-done.49), channel_id=1, source_target_pairs={{0,1},{1,0},{2,3},{3,2},{4,5},{5,4},{6,7},{7,6},{8,9},{9,8},{10,11... | collective-permute-start | bytes 1179656 | tf_op jit(solution)/shard_map/ppermute | solution.py:70
  342.2 1.8 collective-permute-start.51
  342.6 2.8 collective-permute-start.53
  344.1 11.4 %collective-permute-start.52 = (bf16[384,512]{1,0:T(8,128)(2,1)S(1)}, bf16[384,512]{1,0:T(8,128)(2,1)S(1)}, u32[]{:S(2)}, u32[]{:S(2)}) collective-permute-start(bf16[384,512]{1,0:T(8,128)(2,1)S(1)} %add_convert_fusion.1), channel_id=1, source_target_pairs={{0,2},{1,3},{2,0},{3,1},{4,6},{5,7},{6,4},{7,5},{8,10},{9,11},{10,... | collective-permute-start | bytes 1179656 | tf_op jit(solution)/shard_map/ppermute | solution.py:87
  (40 other events, 136.9 us)
where the time goes:
time: 358 us; the launch traced here: 357 us
  waiting for transfers between devices  181 us (51%)
  local copies, waits for them, and re-layouts  57.1 us (16%)
  starting transfers between devices  46.8 us (13%)
  matrix products  42.7 us (12%)
  blocking collectives  21.1 us (6%)
  other arithmetic  6.21 us (2%)
    ppermute x18, waiting for transfers between devices, pieces_of(): current = lax.ppermute(current, 'fs', shift(n_fs, 1))  114 us
    ppermute x18, waiting for transfers between devices, pieces_of(): lax.ppermute(current, 'grp', shift(n_grp, k))  38.5 us
    dynamic_update_slice x23, local copies, waits for them, and re-layouts, absolute(): whole = lax.dynamic_update_slice(whole, part, start)  33.3 us
    ppermute x18, starting transfers between devices, pieces_of(): lax.ppermute(current, 'grp', shift(n_grp, k))  22.2 us
    all_gather x3, blocking collectives, norm_rows(): gain_whole = lax.all_gather(gain, 'tp', axis=1, tiled=True)  21.1 us
    dot_general x32, matrix products, project(): jnp.dot(inputs[s], gathered[s][k], preferred_element_type=jnp.float32)  20.7 us
    ppermute x18, starting transfers between devices, pieces_of(): current = lax.ppermute(current, 'fs', shift(n_fs, 1))  15.6 us
    ppermute x3, waiting for transfers between devices, gather_tp(): far = lax.ppermute(value, 'tp', shift(n_tp, 2 * k))  14.2 us
  transfers between devices with their start and end apart: 54, of which 20 were waited for; matrix products, arithmetic and copies ran while one was open for 20% of the time, Pallas kernels for 0%

commit v1 on v0

--- a/solution.py
+++ b/solution.py
@@ -92,7 +92,24 @@
 
     def norm_rows(values, gain):
         whole = gather_tp(values)
-        gain_whole = lax.all_gather(gain, "tp", axis=1, tiled=True)
+        size_2, index_2, rows_2 = (lax.axis_size("tp"), lax.axis_index("tp"), gain.shape[1])
+        right = [(i_2, (i_2 + 1) % size_2) for i_2 in range(size_2)]
+        left = [(i_2, (i_2 - 1) % size_2) for i_2 in range(size_2)]
+        out_2 = jnp.zeros((*gain.shape[:1], size_2 * rows_2, *gain.shape[1 + 1 :]), gain.dtype)
+        out_2 = lax.dynamic_update_slice_in_dim(out_2, gain, index_2 * rows_2, axis=1)
+        from_left = from_right = gain
+        halfway = size_2 // 2
+        for step_2 in range(1, halfway + 1):
+            from_left = lax.ppermute(from_left, "tp", right)
+            out_2 = lax.dynamic_update_slice_in_dim(
+                out_2, from_left, (index_2 - step_2) % size_2 * rows_2, axis=1
+            )
+            if step_2 < size_2 - halfway:
+                from_right = lax.ppermute(from_right, "tp", left)
+                out_2 = lax.dynamic_update_slice_in_dim(
+                    out_2, from_right, (index_2 + step_2) % size_2 * rows_2, axis=1
+                )
+        gain_whole = out_2
         widened = whole.astype(jnp.float32)
         scaled = (widened * gain_whole.astype(jnp.float32)).astype(jnp.bfloat16)
         factor = lax.rsqrt(jnp.mean(widened * widened, axis=1, keepdims=True) + 1e-06)

time: 358 us -> 369 us (1.031)
  blocking collectives: 21.1 us -> 0 us
  local copies, waits for them, and re-layouts: 57.1 us -> 71.9 us
  other arithmetic: 6.21 us -> 14 us
  starting transfers between devices: 46.8 us -> 54 us
    all_gather x3 -> x0, blocking collectives: 21.1 us -> none  [norm_rows(): gain_whole = lax.all_gather(gain, 'tp', axis=1, tiled=True)]
    dynamic_update_slice x10, local copies, waits for them, and re-layouts: 3.43 us -> 11.8 us  [gather_tp(): whole = lax.dynamic_update_slice(whole, piece, (0, source * value.shape[1]))]
    ppermute x0 -> x9, waiting for transfers between devices: none -> 7.61 us  [the longest x3 4.12 us: norm_rows(): from_right = lax.ppermute(from_right, 'tp', left)]
    ppermute x0 -> x9, starting transfers between devices: none -> 6.4 us  [the longest x6 3.59 us: norm_rows(): from_left = lax.ppermute(from_left, 'tp', right)]
    ppermute x18, waiting for transfers between devices: 114 us -> 109 us  [pieces_of(): current = lax.ppermute(current, 'fs', shift(n_fs, 1))]
    ppermute x0 -> x9, other arithmetic: none -> 4.23 us  [the longest x6 2.16 us: norm_rows(): from_left = lax.ppermute(from_left, 'tp', right)]
    unnamed x100 -> x106, local copies, waits for them, and re-layouts: 10.8 us -> 13 us
  transfers between devices with their start and end apart: 54 -> 63, of which waited for: 20 -> 25; matrix products, arithmetic and copies ran while one was open for 20% -> 25% of each run, Pallas kernels for 0% -> 0%
where the time goes in v1:
time: 369 us; the launch traced here: 368 us
  waiting for transfers between devices  184 us (50%)
  local copies, waits for them, and re-layouts  71.9 us (19%)
  starting transfers between devices  54 us (15%)
  matrix products  42 us (11%)
  other arithmetic  14 us (4%)
    ppermute x18, waiting for transfers between devices, pieces_of(): current = lax.ppermute(current, 'fs', shift(n_fs, 1))  109 us
    ppermute x18, waiting for transfers between devices, pieces_of(): lax.ppermute(current, 'grp', shift(n_grp, k))  40.1 us
    dynamic_update_slice x23, local copies, waits for them, and re-layouts, absolute(): whole = lax.dynamic_update_slice(whole, part, start)  32.5 us
    ppermute x18, starting transfers between devices, pieces_of(): lax.ppermute(current, 'grp', shift(n_grp, k))  21.6 us
    dot_general x32, matrix products, project(): jnp.dot(inputs[s], gathered[s][k], preferred_element_type=jnp.float32)  20.8 us
    ppermute x18, starting transfers between devices, pieces_of(): current = lax.ppermute(current, 'fs', shift(n_fs, 1))  16.3 us
    ppermute x3, waiting for transfers between devices, gather_tp(): far = lax.ppermute(value, 'tp', shift(n_tp, 2 * k))  13.3 us
    ppermute x3, waiting for transfers between devices, scatter_tp(): lax.ppermute(pair.astype(jnp.bfloat16), 'tp', shift(n_tp, 2 * k))  13.1 us
  transfers between devices with their start and end apart: 63, of which 25 were waited for; matrix products, arithmetic and copies ran while one was open for 25% of the time, Pallas kernels for 0%

profile of v1, /device:TPU:0, one launch (start us, length us, event | category | flops | bytes accessed | tf_op | source)
XLA Modules:
  0.0 367.5 jit_solution(2295992860970621199)
XLA Ops:
  0.0 3.0 collective-permute-start.1
  4.2 1.6 collective-permute-start.6
  8.9 3.6 collective-permute-done.1
  16.7 1.8 collective-permute-start.9
  19.5 1.6 collective-permute-start.18
  22.1 1.8 constant_dynamic-update-slice_fusion.24
  23.9 1.8 constant_dynamic-update-slice_fusion.23
  28.8 1.8 constant_dynamic-update-slice_fusion.22
  30.6 2.0 fusion
  33.5 9.9 %collective-permute-done.9 = bf16[512,768]{1,0:T(8,128)(2,1)} collective-permute-done((bf16[512,768]{1,0:T(8,128)(2,1)S(1)}, bf16[512,768]{1,0:T(8,128)(2,1)}, u32[]{:S(2)}, u32[]{:S(2)}) %collective-permute-start.9) | collective-permute-done | bytes 786464 | tf_op jit(solution)/shard_map/ppermute | solution.py:45
  43.5 1.6 fusion.128
  45.6 1.7 fusion.126
  47.8 1.6 collective-permute-start.15
  49.4 10.9 %collective-permute-done.18 = bf16[768,512]{1,0:T(8,128)(2,1)} collective-permute-done((bf16[768,512]{1,0:T(8,128)(2,1)}, bf16[768,512]{1,0:T(8,128)(2,1)}, u32[]{:S(2)}, u32[]{:S(2)}) %collective-permute-start.18) | collective-permute-done | bytes 786464 | tf_op jit(solution)/shard_map/ppermute | solution.py:45
  61.9 15.1 %collective-permute-done.7 = bf16[512,768]{1,0:T(8,128)(2,1)S(1)} collective-permute-done((bf16[512,768]{1,0:T(8,128)(2,1)}, bf16[512,768]{1,0:T(8,128)(2,1)S(1)}, u32[]{:S(2)}, u32[]{:S(2)}) %collective-permute-start.7) | collective-permute-done | bytes 786464 | tf_op jit(solution)/shard_map/ppermute | solution.py:45
  79.5 14.4 %collective-permute-done.10 = bf16[512,768]{1,0:T(8,128)(2,1)S(1)} collective-permute-done((bf16[512,768]{1,0:T(8,128)(2,1)}, bf16[512,768]{1,0:T(8,128)(2,1)S(1)}, u32[]{:S(2)}, u32[]{:S(2)}) %collective-permute-start.10) | collective-permute-done | bytes 786464 | tf_op jit(solution)/shard_map/ppermute | solution.py:45
  96.3 14.5 %collective-permute-done.20 = bf16[768,512]{1,0:T(8,128)(2,1)S(1)} collective-permute-done((bf16[768,512]{1,0:T(8,128)(2,1)}, bf16[768,512]{1,0:T(8,128)(2,1)S(1)}, u32[]{:S(2)}, u32[]{:S(2)}) %collective-permute-start.20) | collective-permute-done | bytes 786464 | tf_op jit(solution)/shard_map/ppermute | solution.py:45
  110.8 1.5 collective-permute-start.16
  113.4 14.2 %collective-permute-done.8 = bf16[512,768]{1,0:T(8,128)(2,1)S(1)} collective-permute-done((bf16[512,768]{1,0:T(8,128)(2,1)S(1)}, bf16[512,768]{1,0:T(8,128)(2,1)S(1)}, u32[]{:S(2)}, u32[]{:S(2)}) %collective-permute-start.8) | collective-permute-done | bytes 786464 | tf_op jit(solution)/shard_map/ppermute | solution.py:45
  128.2 16.3 %collective-permute-done.11 = bf16[512,768]{1,0:T(8,128)(2,1)S(1)} collective-permute-done((bf16[512,768]{1,0:T(8,128)(2,1)S(1)}, bf16[512,768]{1,0:T(8,128)(2,1)S(1)}, u32[]{:S(2)}, u32[]{:S(2)}) %collective-permute-start.11) | collective-permute-done | bytes 786464 | tf_op jit(solution)/shard_map/ppermute | solution.py:45
  144.5 1.5 collective-permute-start.14
  147.1 1.6 fusion.199
  149.2 10.8 %collective-permute-done.22 = bf16[768,512]{1,0:T(8,128)(2,1)S(1)} collective-permute-done((bf16[768,512]{1,0:T(8,128)(2,1)S(1)}, bf16[768,512]{1,0:T(8,128)(2,1)S(1)}, u32[]{:S(2)}, u32[]{:S(2)}) %collective-permute-start.22) | collective-permute-done | bytes 786464 | tf_op jit(solution)/shard_map/ppermute | solution.py:45
  164.0 16.4 %collective-permute-done.17 = bf16[512,768]{1,0:T(8,128)(2,1)S(1)} collective-permute-done((bf16[512,768]{1,0:T(8,128)(2,1)S(1)}, bf16[512,768]{1,0:T(8,128)(2,1)S(1)}, u32[]{:S(2)}, u32[]{:S(2)}) %collective-permute-start.17) | collective-permute-done | bytes 786464 | tf_op jit(solution)/shard_map/ppermute | solution.py:47
  183.0 12.1 %collective-permute-done.23 = bf16[768,512]{1,0:T(8,128)(2,1)S(1)} collective-permute-done((bf16[768,512]{1,0:T(8,128)(2,1)S(1)}, bf16[768,512]{1,0:T(8,128)(2,1)S(1)}, u32[]{:S(2)}, u32[]{:S(2)}) %collective-permute-start.23) | collective-permute-done | bytes 786464 | tf_op jit(solution)/shard_map/ppermute | solution.py:47
  198.7 1.6 constant_dynamic-update-slice_fusion.10
  202.0 1.6 constant_dynamic-slice_fusion.3
  204.5 1.6 dynamic-slice_dynamic-update-slice_fusion.1
  206.3 2.0 add_convert_fusion.4
  209.7 1.6 dynamic-slice_dynamic-update-slice_fusion.2
  214.5 4.1 %collective-permute-done.31 = bf16[1,512]{1,0:T(2,128)(2,1)S(1)} collective-permute-done((bf16[1,512]{1,0:T(2,128)(2,1)S(1)}, bf16[1,512]{1,0:T(2,128)(2,1)S(1)}, u32[]{:S(2)}, u32[]{:S(2)}) %collective-permute-start.31) | collective-permute-done | bytes 1056 | tf_op jit(solution)/shard_map/ppermute | solution.py:108
  222.2 1.6 collective-permute-start.33
  224.7 1.5 collective-permute-start.40
  226.2 2.2 collective-permute-start.41
  231.9 1.6 constant_dynamic-update-slice_fusion.9
  233.5 2.9 dynamic_update_slice.218
  237.7 2.5 collective-permute-start.43
  241.8 2.0 dynamic_update_slice.219
  243.8 3.5 dynamic_update_slice.220
  251.3 2.3 collective-permute-done.48
  254.9 2.1 dynamic_update_slice.221
  257.0 3.4 dynamic_update_slice.222
  260.4 2.1 dynamic_update_slice.223
  264.6 2.5 fusion.61
  267.1 2.0 fusion.138
  269.1 2.0 fusion.143
  271.1 2.1 convolution_convert_fusion
  273.3 3.3 collective-permute-start.34
  277.4 1.7 constant_dynamic-update-slice_fusion.16
  279.2 4.9 %collective-permute-done.34 = bf16[256,512]{1,0:T(8,128)(2,1)S(1)} collective-permute-done((bf16[256,512]{1,0:T(8,128)(2,1)}, bf16[256,512]{1,0:T(8,128)(2,1)S(1)}, u32[]{:S(2)}, u32[]{:S(2)}) %collective-permute-start.34) | collective-permute-done | bytes 262176 | tf_op jit(solution)/shard_map/ppermute | solution.py:47
  284.8 2.1 collective-permute-done.37
  291.1 3.9 %collective-permute-done.38 = bf16[256,512]{1,0:T(8,128)(2,1)S(1)} collective-permute-done((bf16[256,512]{1,0:T(8,128)(2,1)S(1)}, bf16[256,512]{1,0:T(8,128)(2,1)S(1)}, u32[]{:S(2)}, u32[]{:S(2)}) %collective-permute-start.38) | collective-permute-done | bytes 262176 | tf_op jit(solution)/shard_map/ppermute | solution.py:47
  295.8 3.1 collective-permute-done.52
  299.1 2.8 constant_dynamic-update-slice_fusion.3
  304.2 9.7 %collective-permute-done.55 = bf16[384,512]{1,0:T(8,128)(2,1)} collective-permute-done((bf16[384,512]{1,0:T(8,128)(2,1)S(1)}, bf16[384,512]{1,0:T(8,128)(2,1)}, u32[]{:S(2)}, u32[]{:S(2)}) %collective-permute-start.55) | collective-permute-done | bytes 393248 | tf_op jit(solution)/shard_map/ppermute | solution.py:67
  318.3 1.6 collective-permute-done.59
  320.9 1.8 constant_dynamic-update-slice_fusion.2
  322.7 1.8 constant_dynamic-update-slice_fusion.1
  324.5 1.8 constant_dynamic-update-slice_fusion
  326.3 2.1 fusion.4
  331.3 1.7 fusion.104
  334.6 1.7 fusion.102
  346.6 1.7 fusion.203
  356.5 10.0 %collective-permute-done.61 = bf16[384,512]{1,0:T(8,128)(2,1)S(1)} collective-permute-done((bf16[384,512]{1,0:T(8,128)(2,1)S(1)}, bf16[384,512]{1,0:T(8,128)(2,1)S(1)}, u32[]{:S(2)}, u32[]{:S(2)}) %collective-permute-start.61) | collective-permute-done | bytes 393248 | tf_op jit(solution)/shard_map/ppermute | solution.py:87
  (312 shorter events, 98.9 us)
Async XLA Ops:
  0.0 12.5 %collective-permute-start.1 = (bf16[384,512]{1,0:T(8,128)(2,1)}, bf16[384,512]{1,0:T(8,128)(2,1)}, u32[]{:S(2)}, u32[]{:S(2)}) collective-permute-start(bf16[384,512]{1,0:T(8,128)(2,1)} %param.12), channel_id=1, source_target_pairs={{0,2},{1,3},{2,0},{3,1},{4,6},{5,7},{6,4},{7,5},{8,10},{9,11},{10,... | collective-permute-start | bytes 1179656 | tf_op jit(solution)/shard_map/ppermute | solution.py:67
  4.2 22.4 %collective-permute-start.6 = (bf16[512,768]{1,0:T(8,128)(2,1)S(1)}, bf16[512,768]{1,0:T(8,128)(2,1)}, u32[]{:S(2)}, u32[]{:S(2)}) collective-permute-start(bf16[512,768]{1,0:T(8,128)(2,1)S(1)} %constant_dynamic-slice_fusion.11), channel_id=1, source_target_pairs={{0,4},{4,8},{8,12},{12,0},{1,5},{5,9},{9,13},{13,1},{2,6},{6,10},{... | collective-permute-start | bytes 2359304 | tf_op jit(solution)/shard_map/ppermute | solution.py:45
  5.9 16.2 %collective-permute-start = (bf16[384,512]{1,0:T(8,128)(2,1)S(1)}, bf16[384,512]{1,0:T(8,128)(2,1)}, u32[]{:S(2)}, u32[]{:S(2)}) collective-permute-start(bf16[384,512]{1,0:T(8,128)(2,1)S(1)} %copy-done.37), channel_id=1, source_target_pairs={{0,1},{1,0},{2,3},{3,2},{4,5},{5,4},{6,7},{7,6},{8,9},{9,8},{10,11... | collective-permute-start | bytes 1179656 | tf_op jit(solution)/shard_map/ppermute | solution.py:65
  5.9 9.8 %collective-permute-start.3 = (bf16[1,512]{1,0:T(2,128)(2,1)S(1)}, bf16[1,512]{1,0:T(2,128)(2,1)S(1)}, u32[]{:S(2)}, u32[]{:S(2)}) collective-permute-start(bf16[1,512]{1,0:T(2,128)(2,1)S(1)} %copy-done.42), channel_id=1, source_target_pairs={{0,1},{1,2},{2,3},{3,0},{4,5},{5,6},{6,7},{7,4},{8,9},{9,10},{10,1... | collective-permute-start | bytes 3080 | tf_op jit(solution)/shard_map/ppermute | solution.py:103
  6.4 10.4 %collective-permute-start.4 = (bf16[1,512]{1,0:T(2,128)(2,1)S(1)}, bf16[1,512]{1,0:T(2,128)(2,1)}, u32[]{:S(2)}, u32[]{:S(2)}) collective-permute-start(bf16[1,512]{1,0:T(2,128)(2,1)S(1)} %copy-done.42), channel_id=1, source_target_pairs={{0,3},{1,0},{2,1},{3,2},{4,7},{5,4},{6,5},{7,6},{8,11},{9,8},{10,9... | collective-permute-start | bytes 3080 | tf_op jit(solution)/shard_map/ppermute | solution.py:108
  12.5 16.3 %collective-permute-start.2 = (bf16[384,512]{1,0:T(8,128)(2,1)}, bf16[384,512]{1,0:T(8,128)(2,1)}, u32[]{:S(2)}, u32[]{:S(2)}) collective-permute-start(bf16[384,512]{1,0:T(8,128)(2,1)} %collective-permute-done.1), channel_id=1, source_target_pairs={{0,1},{1,0},{2,3},{3,2},{4,5},{5,4},{6,7},{7,6},{8,9},{9,8},{10,11... | collective-permute-start | bytes 1179656 | tf_op jit(solution)/shard_map/ppermute | solution.py:70
  15.7 3.8 %collective-permute-start.5 = (bf16[1,512]{1,0:T(2,128)(2,1)S(1)}, bf16[1,512]{1,0:T(2,128)(2,1)}, u32[]{:S(2)}, u32[]{:S(2)}) collective-permute-start(bf16[1,512]{1,0:T(2,128)(2,1)S(1)} %collective-permute-done.3), channel_id=1, source_target_pairs={{0,1},{1,2},{2,3},{3,0},{4,5},{5,6},{6,7},{7,4},{8,9},{9,10},{10,1... | collective-permute-start | bytes 3080 | tf_op jit(solution)/shard_map/ppermute | solution.py:103
  16.7 26.7 %collective-permute-start.9 = (bf16[512,768]{1,0:T(8,128)(2,1)S(1)}, bf16[512,768]{1,0:T(8,128)(2,1)}, u32[]{:S(2)}, u32[]{:S(2)}) collective-permute-start(bf16[512,768]{1,0:T(8,128)(2,1)S(1)} %constant_dynamic-slice_fusion.10), channel_id=1, source_target_pairs={{0,4},{4,8},{8,12},{12,0},{1,5},{5,9},{9,13},{13,1},{2,6},{6,10},{... | collective-permute-start | bytes 2359304 | tf_op jit(solution)/shard_map/ppermute | solution.py:45
  19.5 40.8 %collective-permute-start.18 = (bf16[768,512]{1,0:T(8,128)(2,1)}, bf16[768,512]{1,0:T(8,128)(2,1)}, u32[]{:S(2)}, u32[]{:S(2)}) collective-permute-start(bf16[768,512]{1,0:T(8,128)(2,1)} %constant_dynamic-slice_fusion.9), channel_id=1, source_target_pairs={{0,4},{4,8},{8,12},{12,0},{1,5},{5,9},{9,13},{13,1},{2,6},{6,10},{... | collective-permute-start | bytes 2359304 | tf_op jit(solution)/shard_map/ppermute | solution.py:45
  26.6 35.2 %collective-permute-start.12 = (bf16[512,768]{1,0:T(8,128)(2,1)}, bf16[512,768]{1,0:T(8,128)(2,1)S(1)}, u32[]{:S(2)}, u32[]{:S(2)}) collective-permute-start(bf16[512,768]{1,0:T(8,128)(2,1)} %collective-permute-done.6), channel_id=1, source_target_pairs={{0,16},{16,0},{1,17},{17,1},{2,18},{18,2},{3,19},{19,3},{4,20},{20... | collective-permute-start | bytes 2359304 | tf_op jit(solution)/shard_map/ppermute | solution.py:47
  28.1 48.9 %collective-permute-start.7 = (bf16[512,768]{1,0:T(8,128)(2,1)}, bf16[512,768]{1,0:T(8,128)(2,1)S(1)}, u32[]{:S(2)}, u32[]{:S(2)}) collective-permute-start(bf16[512,768]{1,0:T(8,128)(2,1)} %collective-permute-done.6), channel_id=1, source_target_pairs={{0,4},{4,8},{8,12},{12,0},{1,5},{5,9},{9,13},{13,1},{2,6},{6,10},{... | collective-permute-start | bytes 2359304 | tf_op jit(solution)/shard_map/ppermute | solution.py:45
  43.5 50.5 %collective-permute-start.10 = (bf16[512,768]{1,0:T(8,128)(2,1)}, bf16[512,768]{1,0:T(8,128)(2,1)S(1)}, u32[]{:S(2)}, u32[]{:S(2)}) collective-permute-start(bf16[512,768]{1,0:T(8,128)(2,1)} %collective-permute-done.9), channel_id=1, source_target_pairs={{0,4},{4,8},{8,12},{12,0},{1,5},{5,9},{9,13},{13,1},{2,6},{6,10},{... | collective-permute-start | bytes 2359304 | tf_op jit(solution)/shard_map/ppermute | solution.py:45
  47.8 46.6 %collective-permute-start.15 = (bf16[512,768]{1,0:T(8,128)(2,1)}, bf16[512,768]{1,0:T(8,128)(2,1)S(1)}, u32[]{:S(2)}, u32[]{:S(2)}) collective-permute-start(bf16[512,768]{1,0:T(8,128)(2,1)} %collective-permute-done.9), channel_id=1, source_target_pairs={{0,16},{16,0},{1,17},{17,1},{2,18},{18,2},{3,19},{19,3},{4,20},{20... | collective-permute-start | bytes 2359304 | tf_op jit(solution)/shard_map/ppermute | solution.py:47
  60.3 121.7 %collective-permute-start.19 = (bf16[768,512]{1,0:T(8,128)(2,1)}, bf16[768,512]{1,0:T(8,128)(2,1)S(1)}, u32[]{:S(2)}, u32[]{:S(2)}) collective-permute-start(bf16[768,512]{1,0:T(8,128)(2,1)} %collective-permute-done.18), channel_id=1, source_target_pairs={{0,16},{16,0},{1,17},{17,1},{2,18},{18,2},{3,19},{19,3},{4,20},{20... | collective-permute-start | bytes 2359304 | tf_op jit(solution)/shard_map/ppermute | solution.py:47
  61.8 48.9 %collective-permute-start.20 = (bf16[768,512]{1,0:T(8,128)(2,1)}, bf16[768,512]{1,0:T(8,128)(2,1)S(1)}, u32[]{:S(2)}, u32[]{:S(2)}) collective-permute-start(bf16[768,512]{1,0:T(8,128)(2,1)} %collective-permute-done.18), channel_id=1, source_target_pairs={{0,4},{4,8},{8,12},{12,0},{1,5},{5,9},{9,13},{13,1},{2,6},{6,10},{... | collective-permute-start | bytes 2359304 | tf_op jit(solution)/shard_map/ppermute | solution.py:45
  77.1 35.2 %collective-permute-start.13 = (bf16[512,768]{1,0:T(8,128)(2,1)S(1)}, bf16[512,768]{1,0:T(8,128)(2,1)S(1)}, u32[]{:S(2)}, u32[]{:S(2)}) collective-permute-start(bf16[512,768]{1,0:T(8,128)(2,1)S(1)} %collective-permute-done.7), channel_id=1, source_target_pairs={{0,16},{16,0},{1,17},{17,1},{2,18},{18,2},{3,19},{19,3},{4,20},{20... | collective-permute-start | bytes 2359304 | tf_op jit(solution)/shard_map/ppermute | solution.py:47
  93.9 33.7 %collective-permute-start.8 = (bf16[512,768]{1,0:T(8,128)(2,1)S(1)}, bf16[512,768]{1,0:T(8,128)(2,1)S(1)}, u32[]{:S(2)}, u32[]{:S(2)}) collective-permute-start(bf16[512,768]{1,0:T(8,128)(2,1)S(1)} %collective-permute-done.7), channel_id=1, source_target_pairs={{0,4},{4,8},{8,12},{12,0},{1,5},{5,9},{9,13},{13,1},{2,6},{6,10},{... | collective-permute-start | bytes 2359304 | tf_op jit(solution)/shard_map/ppermute | solution.py:45
  94.4 50.1 %collective-permute-start.11 = (bf16[512,768]{1,0:T(8,128)(2,1)S(1)}, bf16[512,768]{1,0:T(8,128)(2,1)S(1)}, u32[]{:S(2)}, u32[]{:S(2)}) collective-permute-start(bf16[512,768]{1,0:T(8,128)(2,1)S(1)} %collective-permute-done.10), channel_id=1, source_target_pairs={{0,4},{4,8},{8,12},{12,0},{1,5},{5,9},{9,13},{13,1},{2,6},{6,10},{... | collective-permute-start | bytes 2359304 | tf_op jit(solution)/shard_map/ppermute | solution.py:45
  110.8 38.0 %copy-start.25 = (bf16[768,512]{1,0:T(8,128)(2,1)}, bf16[768,512]{1,0:T(8,128)(2,1)S(1)}, u32[]{:S(2)}) copy-start(bf16[768,512]{1,0:T(8,128)(2,1)S(1)} %collective-permute-done.20) | copy-start | bytes 2359300
  110.8 51.2 %collective-permute-start.16 = (bf16[512,768]{1,0:T(8,128)(2,1)S(1)}, bf16[512,768]{1,0:T(8,128)(2,1)S(1)}, u32[]{:S(2)}, u32[]{:S(2)}) collective-permute-start(bf16[512,768]{1,0:T(8,128)(2,1)S(1)} %collective-permute-done.10), channel_id=1, source_target_pairs={{0,16},{16,0},{1,17},{17,1},{2,18},{18,2},{3,19},{19,3},{4,20},{20... | collective-permute-start | bytes 2359304 | tf_op jit(solution)/shard_map/ppermute | solution.py:47
  112.3 70.2 %collective-permute-start.21 = (bf16[768,512]{1,0:T(8,128)(2,1)S(1)}, bf16[768,512]{1,0:T(8,128)(2,1)S(1)}, u32[]{:S(2)}, u32[]{:S(2)}) collective-permute-start(bf16[768,512]{1,0:T(8,128)(2,1)S(1)} %collective-permute-done.20), channel_id=1, source_target_pairs={{0,16},{16,0},{1,17},{17,1},{2,18},{18,2},{3,19},{19,3},{4,20},{20... | collective-permute-start | bytes 2359304 | tf_op jit(solution)/shard_map/ppermute | solution.py:47
  127.6 32.4 %collective-permute-start.22 = (bf16[768,512]{1,0:T(8,128)(2,1)S(1)}, bf16[768,512]{1,0:T(8,128)(2,1)S(1)}, u32[]{:S(2)}, u32[]{:S(2)}) collective-permute-start(bf16[768,512]{1,0:T(8,128)(2,1)S(1)} %collective-permute-done.20), channel_id=1, source_target_pairs={{0,4},{4,8},{8,12},{12,0},{1,5},{5,9},{9,13},{13,1},{2,6},{6,10},{... | collective-permute-start | bytes 2359304 | tf_op jit(solution)/shard_map/ppermute | solution.py:45
  144.5 18.6 %collective-permute-start.14 = (bf16[512,768]{1,0:T(8,128)(2,1)S(1)}, bf16[512,768]{1,0:T(8,128)(2,1)S(1)}, u32[]{:S(2)}, u32[]{:S(2)}) collective-permute-start(bf16[512,768]{1,0:T(8,128)(2,1)S(1)} %collective-permute-done.8), channel_id=1, source_target_pairs={{0,16},{16,0},{1,17},{17,1},{2,18},{18,2},{3,19},{19,3},{4,20},{20... | collective-permute-start | bytes 2359304 | tf_op jit(solution)/shard_map/ppermute | solution.py:47
  160.0 20.4 %collective-permute-start.17 = (bf16[512,768]{1,0:T(8,128)(2,1)S(1)}, bf16[512,768]{1,0:T(8,128)(2,1)S(1)}, u32[]{:S(2)}, u32[]{:S(2)}) collective-permute-start(bf16[512,768]{1,0:T(8,128)(2,1)S(1)} %collective-permute-done.11), channel_id=1, source_target_pairs={{0,16},{16,0},{1,17},{17,1},{2,18},{18,2},{3,19},{19,3},{4,20},{20... | collective-permute-start | bytes 2359304 | tf_op jit(solution)/shard_map/ppermute | solution.py:47
  162.0 33.1 %collective-permute-start.23 = (bf16[768,512]{1,0:T(8,128)(2,1)S(1)}, bf16[768,512]{1,0:T(8,128)(2,1)S(1)}, u32[]{:S(2)}, u32[]{:S(2)}) collective-permute-start(bf16[768,512]{1,0:T(8,128)(2,1)S(1)} %collective-permute-done.22), channel_id=1, source_target_pairs={{0,16},{16,0},{1,17},{17,1},{2,18},{18,2},{3,19},{19,3},{4,20},{20... | collective-permute-start | bytes 2359304 | tf_op jit(solution)/shard_map/ppermute | solution.py:47
  197.6 8.6 %collective-permute-start.24 = (bf16[384,512]{1,0:T(8,128)(2,1)}, bf16[384,512]{1,0:T(8,128)(2,1)}, u32[]{:S(2)}, u32[]{:S(2)}) collective-permute-start(bf16[384,512]{1,0:T(8,128)(2,1)} %get-tuple-element.17), channel_id=1, source_target_pairs={{0,1},{1,0},{2,3},{3,2},{4,5},{5,4},{6,7},{7,6},{8,9},{9,8},{10,11... | collective-permute-start | bytes 1179656 | tf_op jit(solution)/shard_map/ppermute | solution.py:84
  200.3 24.4 %collective-permute-start.39 = (bf16[256,256]{1,0:T(8,128)(2,1)}, bf16[256,256]{1,0:T(8,128)(2,1)}, u32[]{:S(2)}, u32[]{:S(2)}) collective-permute-start(bf16[256,256]{1,0:T(8,128)(2,1)} %get-tuple-element.6), channel_id=1, source_target_pairs={{0,4},{4,8},{8,12},{12,0},{1,5},{5,9},{9,13},{13,1},{2,6},{6,10},{... | collective-permute-start | bytes 393224 | tf_op jit(solution)/shard_map/ppermute | solution.py:45
  200.4 13.2 %collective-permute-start.30 = (bf16[1,512]{1,0:T(2,128)(2,1)S(1)}, bf16[1,512]{1,0:T(2,128)(2,1)S(1)}, u32[]{:S(2)}, u32[]{:S(2)}) collective-permute-start(bf16[1,512]{1,0:T(2,128)(2,1)S(1)} %copy-done.43), channel_id=1, source_target_pairs={{0,1},{1,2},{2,3},{3,0},{4,5},{5,6},{6,7},{7,4},{8,9},{9,10},{10,1... | collective-permute-start | bytes 3080 | tf_op jit(solution)/shard_map/ppermute | solution.py:103
  203.6 22.6 %collective-permute-start.45 = (bf16[128,512]{1,0:T(8,128)(2,1)}, bf16[128,512]{1,0:T(8,128)(2,1)}, u32[]{:S(2)}, u32[]{:S(2)}) collective-permute-start(bf16[128,512]{1,0:T(8,128)(2,1)} %get-tuple-element.21), channel_id=1, source_target_pairs={{0,4},{4,8},{8,12},{12,0},{1,5},{5,9},{9,13},{13,1},{2,6},{6,10},{... | collective-permute-start | bytes 393224 | tf_op jit(solution)/shard_map/ppermute | solution.py:45
  206.1 22.3 %collective-permute-start.26 = (bf16[384,512]{1,0:T(8,128)(2,1)}, bf16[384,512]{1,0:T(8,128)(2,1)}, u32[]{:S(2)}, u32[]{:S(2)}) collective-permute-start(bf16[384,512]{1,0:T(8,128)(2,1)} %get-tuple-element.18), channel_id=1, source_target_pairs={{0,1},{1,0},{2,3},{3,2},{4,5},{5,4},{6,7},{7,6},{8,9},{9,8},{10,11... | collective-permute-start | bytes 1179656 | tf_op jit(solution)/shard_map/ppermute | solution.py:84
  208.2 20.7 %collective-permute-start.25 = (bf16[384,512]{1,0:T(8,128)(2,1)}, bf16[384,512]{1,0:T(8,128)(2,1)}, u32[]{:S(2)}, u32[]{:S(2)}) collective-permute-start(bf16[384,512]{1,0:T(8,128)(2,1)} %add_convert_fusion.4), channel_id=1, source_target_pairs={{0,2},{1,3},{2,0},{3,1},{4,6},{5,7},{6,4},{7,5},{8,10},{9,11},{10,... | collective-permute-start | bytes 1179656 | tf_op jit(solution)/shard_map/ppermute | solution.py:87
  213.6 5.0 %collective-permute-start.31 = (bf16[1,512]{1,0:T(2,128)(2,1)S(1)}, bf16[1,512]{1,0:T(2,128)(2,1)S(1)}, u32[]{:S(2)}, u32[]{:S(2)}) collective-permute-start(bf16[1,512]{1,0:T(2,128)(2,1)S(1)} %copy-done.43), channel_id=1, source_target_pairs={{0,3},{1,0},{2,1},{3,2},{4,7},{5,4},{6,5},{7,6},{8,11},{9,8},{10,9... | collective-permute-start | bytes 3080 | tf_op jit(solution)/shard_map/ppermute | solution.py:108
  218.6 3.6 collective-permute-start.32
  222.2 19.0 %collective-permute-start.33 = (bf16[256,512]{1,0:T(8,128)(2,1)}, bf16[256,512]{1,0:T(8,128)(2,1)}, u32[]{:S(2)}, u32[]{:S(2)}) collective-permute-start(bf16[256,512]{1,0:T(8,128)(2,1)} %get-tuple-element.10), channel_id=1, source_target_pairs={{0,4},{4,8},{8,12},{12,0},{1,5},{5,9},{9,13},{13,1},{2,6},{6,10},{... | collective-permute-start | bytes 786440 | tf_op jit(solution)/shard_map/ppermute | solution.py:45
  224.7 6.2 %collective-permute-start.40 = (bf16[256,256]{1,0:T(8,128)(2,1)}, bf16[256,256]{1,0:T(8,128)(2,1)S(1)}, u32[]{:S(2)}, u32[]{:S(2)}) collective-permute-start(bf16[256,256]{1,0:T(8,128)(2,1)} %collective-permute-done.39), channel_id=1, source_target_pairs={{0,16},{16,0},{1,17},{17,1},{2,18},{18,2},{3,19},{19,3},{4,20},{20... | collective-permute-start | bytes 393224 | tf_op jit(solution)/shard_map/ppermute | solution.py:47
  226.2 10.1 %collective-permute-start.41 = (bf16[256,256]{1,0:T(8,128)(2,1)}, bf16[256,256]{1,0:T(8,128)(2,1)S(1)}, u32[]{:S(2)}, u32[]{:S(2)}) collective-permute-start(bf16[256,256]{1,0:T(8,128)(2,1)} %collective-permute-done.39), channel_id=1, source_target_pairs={{0,4},{4,8},{8,12},{12,0},{1,5},{5,9},{9,13},{13,1},{2,6},{6,10},{... | collective-permute-start | bytes 393224 | tf_op jit(solution)/shard_map/ppermute | solution.py:45
  228.5 9.2 %collective-permute-start.46 = (bf16[128,512]{1,0:T(8,128)(2,1)}, bf16[128,512]{1,0:T(8,128)(2,1)S(1)}, u32[]{:S(2)}, u32[]{:S(2)}) collective-permute-start(bf16[128,512]{1,0:T(8,128)(2,1)} %collective-permute-done.45), channel_id=1, source_target_pairs={{0,16},{16,0},{1,17},{17,1},{2,18},{18,2},{3,19},{19,3},{4,20},{20... | collective-permute-start | bytes 393224 | tf_op jit(solution)/shard_map/ppermute | solution.py:47
  228.9 11.3 %collective-permute-start.47 = (bf16[128,512]{1,0:T(8,128)(2,1)}, bf16[128,512]{1,0:T(8,128)(2,1)S(1)}, u32[]{:S(2)}, u32[]{:S(2)}) collective-permute-start(bf16[128,512]{1,0:T(8,128)(2,1)} %collective-permute-done.45), channel_id=1, source_target_pairs={{0,4},{4,8},{8,12},{12,0},{1,5},{5,9},{9,13},{13,1},{2,6},{6,10},{... | collective-permute-start | bytes 393224 | tf_op jit(solution)/shard_map/ppermute | solution.py:45
  231.0 19.7 %collective-permute-start.28 = (bf16[384,512]{1,0:T(8,128)(2,1)S(1)}, bf16[384,512]{1,0:T(8,128)(2,1)S(1)}, u32[]{:S(2)}, u32[]{:S(2)}) collective-permute-start(bf16[384,512]{1,0:T(8,128)(2,1)S(1)} %get-tuple-element.8), channel_id=1, source_target_pairs={{0,2},{1,3},{2,0},{3,1},{4,6},{5,7},{6,4},{7,5},{8,10},{9,11},{10,... | collective-permute-start | bytes 1179656 | tf_op jit(solution)/shard_map/ppermute | solution.py:67
  236.3 11.0 %collective-permute-start.42 = (bf16[256,256]{1,0:T(8,128)(2,1)S(1)}, bf16[256,256]{1,0:T(8,128)(2,1)S(1)}, u32[]{:S(2)}, u32[]{:S(2)}) collective-permute-start(bf16[256,256]{1,0:T(8,128)(2,1)S(1)} %collective-permute-done.41), channel_id=1, source_target_pairs={{0,16},{16,0},{1,17},{17,1},{2,18},{18,2},{3,19},{19,3},{4,20},{20... | collective-permute-start | bytes 393224 | tf_op jit(solution)/shard_map/ppermute | solution.py:47
  237.7 10.3 %collective-permute-start.43 = (bf16[256,256]{1,0:T(8,128)(2,1)S(1)}, bf16[256,256]{1,0:T(8,128)(2,1)S(1)}, u32[]{:S(2)}, u32[]{:S(2)}) collective-permute-start(bf16[256,256]{1,0:T(8,128)(2,1)S(1)} %collective-permute-done.41), channel_id=1, source_target_pairs={{0,4},{4,8},{8,12},{12,0},{1,5},{5,9},{9,13},{13,1},{2,6},{6,10},{... | collective-permute-start | bytes 393224 | tf_op jit(solution)/shard_map/ppermute | solution.py:45
  240.2 9.1 %collective-permute-start.49 = (bf16[128,512]{1,0:T(8,128)(2,1)S(1)}, bf16[128,512]{1,0:T(8,128)(2,1)S(1)}, u32[]{:S(2)}, u32[]{:S(2)}) collective-permute-start(bf16[128,512]{1,0:T(8,128)(2,1)S(1)} %collective-permute-done.47), channel_id=1, source_target_pairs={{0,4},{4,8},{8,12},{12,0},{1,5},{5,9},{9,13},{13,1},{2,6},{6,10},{... | collective-permute-start | bytes 393224 | tf_op jit(solution)/shard_map/ppermute | solution.py:45
  241.1 22.1 %collective-permute-start.27 = (bf16[384,512]{1,0:T(8,128)(2,1)S(1)}, bf16[384,512]{1,0:T(8,128)(2,1)S(1)}, u32[]{:S(2)}, u32[]{:S(2)}) collective-permute-start(bf16[384,512]{1,0:T(8,128)(2,1)S(1)} %get-tuple-element.8), channel_id=1, source_target_pairs={{0,1},{1,0},{2,3},{3,2},{4,5},{5,4},{6,7},{7,6},{8,9},{9,8},{10,11... | collective-permute-start | bytes 1179656 | tf_op jit(solution)/shard_map/ppermute | solution.py:65
  247.3 6.4 %collective-permute-start.48 = (bf16[128,512]{1,0:T(8,128)(2,1)S(1)}, bf16[128,512]{1,0:T(8,128)(2,1)S(1)}, u32[]{:S(2)}, u32[]{:S(2)}) collective-permute-start(bf16[128,512]{1,0:T(8,128)(2,1)S(1)} %collective-permute-done.47), channel_id=1, source_target_pairs={{0,16},{16,0},{1,17},{17,1},{2,18},{18,2},{3,19},{19,3},{4,20},{20... | collective-permute-start | bytes 393224 | tf_op jit(solution)/shard_map/ppermute | solution.py:47
  248.0 14.5 %collective-permute-start.44 = (bf16[256,256]{1,0:T(8,128)(2,1)S(1)}, bf16[256,256]{1,0:T(8,128)(2,1)S(1)}, u32[]{:S(2)}, u32[]{:S(2)}) collective-permute-start(bf16[256,256]{1,0:T(8,128)(2,1)S(1)} %collective-permute-done.43), channel_id=1, source_target_pairs={{0,16},{16,0},{1,17},{17,1},{2,18},{18,2},{3,19},{19,3},{4,20},{20... | collective-permute-start | bytes 393224 | tf_op jit(solution)/shard_map/ppermute | solution.py:47
  249.3 11.1 %collective-permute-start.50 = (bf16[128,512]{1,0:T(8,128)(2,1)S(1)}, bf16[128,512]{1,0:T(8,128)(2,1)S(1)}, u32[]{:S(2)}, u32[]{:S(2)}) collective-permute-start(bf16[128,512]{1,0:T(8,128)(2,1)S(1)} %collective-permute-done.49), channel_id=1, source_target_pairs={{0,16},{16,0},{1,17},{17,1},{2,18},{18,2},{3,19},{19,3},{4,20},{20... | collective-permute-start | bytes 393224 | tf_op jit(solution)/shard_map/ppermute | solution.py:47
  250.7 12.6 %collective-permute-start.29 = (bf16[384,512]{1,0:T(8,128)(2,1)S(1)}, bf16[384,512]{1,0:T(8,128)(2,1)S(1)}, u32[]{:S(2)}, u32[]{:S(2)}) collective-permute-start(bf16[384,512]{1,0:T(8,128)(2,1)S(1)} %collective-permute-done.28), channel_id=1, source_target_pairs={{0,1},{1,0},{2,3},{3,2},{4,5},{5,4},{6,7},{7,6},{8,9},{9,8},{10,11... | collective-permute-start | bytes 1179656 | tf_op jit(solution)/shard_map/ppermute | solution.py:70
  253.7 23.0 %collective-permute-start.35 = (bf16[256,512]{1,0:T(8,128)(2,1)}, bf16[256,512]{1,0:T(8,128)(2,1)S(1)}, u32[]{:S(2)}, u32[]{:S(2)}) collective-permute-start(bf16[256,512]{1,0:T(8,128)(2,1)} %collective-permute-done.33), channel_id=1, source_target_pairs={{0,4},{4,8},{8,12},{12,0},{1,5},{5,9},{9,13},{13,1},{2,6},{6,10},{... | collective-permute-start | bytes 786440 | tf_op jit(solution)/shard_map/ppermute | solution.py:45
  273.3 13.9 %collective-permute-start.51 = (bf16[384,512]{1,0:T(8,128)(2,1)S(1)}, bf16[384,512]{1,0:T(8,128)(2,1)S(1)}, u32[]{:S(2)}, u32[]{:S(2)}) collective-permute-start(bf16[384,512]{1,0:T(8,128)(2,1)S(1)} %get-tuple-element.15), channel_id=1, source_target_pairs={{0,1},{1,0},{2,3},{3,2},{4,5},{5,4},{6,7},{7,6},{8,9},{9,8},{10,11... | collective-permute-start | bytes 1179656 | tf_op jit(solution)/shard_map/ppermute | solution.py:84
  273.3 10.7 %collective-permute-start.34 = (bf16[256,512]{1,0:T(8,128)(2,1)}, bf16[256,512]{1,0:T(8,128)(2,1)S(1)}, u32[]{:S(2)}, u32[]{:S(2)}) collective-permute-start(bf16[256,512]{1,0:T(8,128)(2,1)} %collective-permute-done.33), channel_id=1, source_target_pairs={{0,16},{16,0},{1,17},{17,1},{2,18},{18,2},{3,19},{19,3},{4,20},{20... | collective-permute-start | bytes 786440 | tf_op jit(solution)/shard_map/ppermute | solution.py:47
  276.7 10.2 %collective-permute-start.37 = (bf16[256,512]{1,0:T(8,128)(2,1)S(1)}, bf16[256,512]{1,0:T(8,128)(2,1)S(1)}, u32[]{:S(2)}, u32[]{:S(2)}) collective-permute-start(bf16[256,512]{1,0:T(8,128)(2,1)S(1)} %collective-permute-done.35), channel_id=1, source_target_pairs={{0,4},{4,8},{8,12},{12,0},{1,5},{5,9},{9,13},{13,1},{2,6},{6,10},{... | collective-permute-start | bytes 786440 | tf_op jit(solution)/shard_map/ppermute | solution.py:45
  279.1 10.6 %collective-permute-start.36 = (bf16[256,512]{1,0:T(8,128)(2,1)S(1)}, bf16[256,512]{1,0:T(8,128)(2,1)S(1)}, u32[]{:S(2)}, u32[]{:S(2)}) collective-permute-start(bf16[256,512]{1,0:T(8,128)(2,1)S(1)} %collective-permute-done.35), channel_id=1, source_target_pairs={{0,16},{16,0},{1,17},{17,1},{2,18},{18,2},{3,19},{19,3},{4,20},{20... | collective-permute-start | bytes 786440 | tf_op jit(solution)/shard_map/ppermute | solution.py:47
  286.8 8.2 %collective-permute-start.38 = (bf16[256,512]{1,0:T(8,128)(2,1)S(1)}, bf16[256,512]{1,0:T(8,128)(2,1)S(1)}, u32[]{:S(2)}, u32[]{:S(2)}) collective-permute-start(bf16[256,512]{1,0:T(8,128)(2,1)S(1)} %collective-permute-done.37), channel_id=1, source_target_pairs={{0,16},{16,0},{1,17},{17,1},{2,18},{18,2},{3,19},{19,3},{4,20},{20... | collective-permute-start | bytes 786440 | tf_op jit(solution)/shard_map/ppermute | solution.py:47
  287.1 8.7 %collective-permute-start.53 = (bf16[384,512]{1,0:T(8,128)(2,1)S(1)}, bf16[384,512]{1,0:T(8,128)(2,1)S(1)}, u32[]{:S(2)}, u32[]{:S(2)}) collective-permute-start(bf16[384,512]{1,0:T(8,128)(2,1)S(1)} %get-tuple-element.16), channel_id=1, source_target_pairs={{0,1},{1,0},{2,3},{3,2},{4,5},{5,4},{6,7},{7,6},{8,9},{9,8},{10,11... | collective-permute-start | bytes 1179656 | tf_op jit(solution)/shard_map/ppermute | solution.py:84
  287.3 11.6 %collective-permute-start.52 = (bf16[384,512]{1,0:T(8,128)(2,1)S(1)}, bf16[384,512]{1,0:T(8,128)(2,1)S(1)}, u32[]{:S(2)}, u32[]{:S(2)}) collective-permute-start(bf16[384,512]{1,0:T(8,128)(2,1)S(1)} %add_convert_fusion.2), channel_id=1, source_target_pairs={{0,2},{1,3},{2,0},{3,1},{4,6},{5,7},{6,4},{7,5},{8,10},{9,11},{10,... | collective-permute-start | bytes 1179656 | tf_op jit(solution)/shard_map/ppermute | solution.py:87
  303.0 10.8 %collective-permute-start.55 = (bf16[384,512]{1,0:T(8,128)(2,1)S(1)}, bf16[384,512]{1,0:T(8,128)(2,1)}, u32[]{:S(2)}, u32[]{:S(2)}) collective-permute-start(bf16[384,512]{1,0:T(8,128)(2,1)S(1)} %get-tuple-element.24), channel_id=1, source_target_pairs={{0,2},{1,3},{2,0},{3,1},{4,6},{5,7},{6,4},{7,5},{8,10},{9,11},{10,... | collective-permute-start | bytes 1179656 | tf_op jit(solution)/shard_map/ppermute | solution.py:67
  304.2 16.7 %collective-permute-start.54 = (bf16[384,512]{1,0:T(8,128)(2,1)S(1)}, bf16[384,512]{1,0:T(8,128)(2,1)}, u32[]{:S(2)}, u32[]{:S(2)}) collective-permute-start(bf16[384,512]{1,0:T(8,128)(2,1)S(1)} %get-tuple-element.24), channel_id=1, source_target_pairs={{0,1},{1,0},{2,3},{3,2},{4,5},{5,4},{6,7},{7,6},{8,9},{9,8},{10,11... | collective-permute-start | bytes 1179656 | tf_op jit(solution)/shard_map/ppermute | solution.py:65
  313.8 10.7 %collective-permute-start.56 = (bf16[384,512]{1,0:T(8,128)(2,1)}, bf16[384,512]{1,0:T(8,128)(2,1)}, u32[]{:S(2)}, u32[]{:S(2)}) collective-permute-start(bf16[384,512]{1,0:T(8,128)(2,1)} %collective-permute-done.55), channel_id=1, source_target_pairs={{0,1},{1,0},{2,3},{3,2},{4,5},{5,4},{6,7},{7,6},{8,9},{9,8},{10,11... | collective-permute-start | bytes 1179656 | tf_op jit(solution)/shard_map/ppermute | solution.py:70
  313.8 3.0 collective-permute-start.57
  314.3 3.1 collective-permute-start.58
  316.8 3.1 collective-permute-start.59
  353.4 1.8 collective-permute-start.60
  353.5 3.0 collective-permute-start.62
  355.3 11.2 %collective-permute-start.61 = (bf16[384,512]{1,0:T(8,128)(2,1)S(1)}, bf16[384,512]{1,0:T(8,128)(2,1)S(1)}, u32[]{:S(2)}, u32[]{:S(2)}) collective-permute-start(bf16[384,512]{1,0:T(8,128)(2,1)S(1)} %add_convert_fusion.1), channel_id=1, source_target_pairs={{0,2},{1,3},{2,0},{3,1},{4,6},{5,7},{6,4},{7,5},{8,10},{9,11},{10,... | collective-permute-start | bytes 1179656 | tf_op jit(solution)/shard_map/ppermute | solution.py:87
  (52 other events, 300.4 us)
